TPU v7x, 32 devices: a whole 2x2x4 slice. The times are simulated.
32 devices in a mesh: sp: 8 (over z, x), tp: 4 (over y, core).
Axes of the slice: x: 2, y: 2, z: 4, core: 2. Of those that a mesh axis runs over, the one named last changes fastest.
Arguments:
- query: bfloat16 [2048, 1024], P('sp', 'tp'), may hold values from -6 to 6
- forget_logits: bfloat16 [2048, 1024], P('sp', 'tp'), may hold values from -5.5 to 5.5
- written_values: bfloat16 [2048, 1024], P('sp', 'tp'), may hold values from -6 to 6
- output_gate_logits: bfloat16 [2048, 1024], P('sp', 'tp'), may hold values from -6 to 6
- forget_floor_gap: float32 [1024], P('tp'), may hold values from 0 to 0.08
- extra_log_decay: float32 [2048, 1024], P('sp', 'tp'), may hold values from -0.7 to 0
- head_norm_gain: float32 [128], replicated, may hold values from 0.1 to 1.9
- output_weight: bfloat16 [1024, 2048], P('tp'), may hold values from -0.1875 to 0.1875
- residual: bfloat16 [2048, 2048], P(('sp', 'tp')), may hold values from -6 to 6
- mixer_norm_gain: float32 [2048], replicated, may hold values from 0.1 to 1.9
- mixer_up_weight: bfloat16 [2048, 8192], P('sp', 'tp'), may hold values from -0.125 to 0.125
- mixer_down_weight: bfloat16 [8192, 2048], P(('tp', 'sp')), may hold values from -0.0625 to 0.0625
Outputs:
- layer_out: bfloat16 [2048, 2048], P(('sp', 'tp'))
All inputs are finite; a program needn't handle non-finite values.
Results may differ from a plain program's by a relative error of at most 0.015.
Values may be sent and summed in bfloat16 or wider, within the bound.
A program may use at most 128 MiB of HBM per device.

v0:
```python
import functools

import jax
import jax.numpy as jnp
from jax import lax
from jax.experimental import pallas as pl
from jax.experimental.pallas import tpu as pltpu
from jax.sharding import PartitionSpec as P

HEAD_K = 128
HEAD_V = 128
BLOCK = 64


norm_eps = 1e-06
highest_precision = lax.Precision.HIGHEST


def carried_in(part, axis, combine, identity):
    place = lax.axis_index(axis)
    gathered = jax.tree.map(lambda a: lax.all_gather(a, axis), part)
    state = jax.tree.map(lambda a, e: jnp.zeros_like(a) + jnp.asarray(e, a.dtype), part, identity)

    def one(step, state):
        return combine(
            state, jax.tree.map(lambda a: lax.dynamic_index_in_dim(a, step, 0, False), gathered)
        )

    return lax.fori_loop(0, place, one, state)


def block_update(carry_forward_state, block_inputs):
    query_rows_block, gate_rows_block, value_rows_block, log_block = block_inputs
    cumulative_log = jnp.cumsum(log_block, axis=1)
    length = query_rows_block.shape[1]
    causal = jnp.arange(length)[:, None] >= jnp.arange(length)[None, :]
    across_blocks = jnp.einsum(
        "dcj,djw->dcw",
        query_rows_block * jnp.exp(cumulative_log),
        carry_forward_state,
        precision=highest_precision,
    )
    spread = cumulative_log[:, :, None, :] - cumulative_log[:, None, :, :]
    decay_table = jnp.exp(jnp.where(causal[None, :, :, None], spread, -jnp.inf))
    scores = jnp.einsum(
        "htk,hsk,htsk->hts",
        query_rows_block,
        gate_rows_block,
        decay_table,
        precision=highest_precision,
    )
    within = jnp.einsum("hts,hsv->htv", scores, value_rows_block, precision=highest_precision)
    final_log_total = cumulative_log[:, -1:, :]
    updated_state = jnp.exp(final_log_total[:, 0, :])[
        :, :, None
    ] * carry_forward_state + jnp.einsum(
        "tri,trw->tiw",
        gate_rows_block * jnp.exp(final_log_total - cumulative_log),
        value_rows_block,
        precision=highest_precision,
    )
    return (updated_state, across_blocks + within)


def to_blocks(array, inner):
    length = array.shape[0]
    split_up = array.reshape(length // BLOCK, BLOCK, array.shape[1] // inner, inner)
    return jnp.transpose(split_up, (0, 2, 1, 3))


def from_blocks(blocked):
    joined = jnp.transpose(blocked, (0, 2, 1, 3))
    return joined.reshape(joined.shape[0] * joined.shape[1], joined.shape[2], joined.shape[3])


def prepare_inputs(query, forget_logits, written_values, forget_floor_gap, extra_log_decay):
    input_gate_value = forget_floor_gap[None, :] * jax.nn.sigmoid(
        -forget_logits.astype(jnp.float32)
    )
    forget_log_rate = jnp.log1p(-input_gate_value) + extra_log_decay
    scaled_values = query.astype(jnp.float32) * HEAD_K ** (-0.5)
    return (scaled_values, input_gate_value, written_values.astype(jnp.float32), forget_log_rate)


def gate_out(recurrent, output_gate_logits, head_norm_gain):
    normal_part = recurrent * lax.rsqrt(
        jnp.mean(recurrent * recurrent, axis=-1, keepdims=True) + norm_eps
    )
    gating = jax.nn.silu(output_gate_logits.astype(jnp.float32)).reshape(recurrent.shape)
    mixed = normal_part * head_norm_gain * gating
    return mixed.reshape(recurrent.shape[0], -1).astype(jnp.bfloat16)


def normalize(stream, gain):
    scaled_rows = stream * lax.rsqrt(jnp.mean(stream * stream, axis=-1, keepdims=True) + norm_eps)
    return (scaled_rows * gain).astype(jnp.bfloat16)


def chain_states(earlier, later):
    return (earlier[0] + later[0], jnp.exp(later[0])[:, :, None] * earlier[1] + later[1])


OUTER = 4
LO = 2
MESH = pl.DeviceIdType.MESH


def mixer_kernel(
    sp_size, tp_size,
    mixed_ref, wo_ref, res_ref, gain_ref, up_ref, down_ref, out_ref,
    pbuf, stream, s5, r5, s6, r6, nb, acc, s1, r1, s2, r2, acc2, s3, r3,
    sem5s, sem5r, sem6s, sem6r, zs, zr, hs, hr, ls, lr, ls2, lr2,
    q1s, q1r, q2s, q2r, q3s, q3r,
):
    outer, inner, hi = OUTER, sp_size // OUTER, tp_size // LO
    sp, tp = lax.axis_index("sp"), lax.axis_index("tp")
    o, i = lax.div(sp, inner), lax.rem(sp, inner)
    h, l = lax.div(tp, LO), lax.rem(tp, LO)
    other = 1 - l
    rows, depth = res_ref.shape

    def dev(oo, hh, ll):
        return (oo * inner + i, hh * LO + ll)

    def at_o(k):
        return lax.rem(o + k, outer)

    def from_o(k):
        return lax.rem(o - k + outer, outer)

    def at_h(m):
        return lax.rem(h + m, hi)

    def from_h(m):
        return lax.rem(h - m + hi, hi)

    def rcopy(src, dst, ssem, rsem, device):
        return pltpu.make_async_remote_copy(
            src_ref=src, dst_ref=dst, send_sem=ssem, recv_sem=rsem,
            device_id=device, device_id_type=MESH,
        )

    barrier = pltpu.get_barrier_semaphore()
    peers = [dev(at_o(k), h, l) for k in range(1, outer)]
    peers += [dev(o, at_h(m), l) for m in range(1, hi)] + [dev(o, h, other)]
    for peer in peers:
        pl.semaphore_signal(barrier, inc=1, device_id=peer, device_id_type=MESH)
    pl.semaphore_wait(barrier, len(peers))

    branch = jnp.dot(mixed_ref[...], wo_ref[...], preferred_element_type=jnp.float32)
    pbuf[...] = branch.reshape(tp_size, rows, depth)
    for hh in range(hi):
        s5[hh] = pbuf[hh * LO + other].astype(jnp.bfloat16)
    c5 = rcopy(s5, r5, sem5s, sem5r, dev(o, h, other))
    c5.start()
    c5.wait_recv()
    c6 = []
    for m in range(1, hi):
        to = at_h(m)
        s6[m] = (pbuf[to * LO + l] + r5[to].astype(jnp.float32)).astype(jnp.bfloat16)
        c = rcopy(s6.at[m], r6.at[m], sem6s.at[m], sem6r.at[m], dev(o, to, l))
        c.start()
        c6.append(c)
    total = pbuf[tp] + r5[h].astype(jnp.float32) + res_ref[...].astype(jnp.float32)
    for m in range(1, hi):
        c6[m - 1].wait_recv()
        total = total + r6[m].astype(jnp.float32)
    stream[...] = total
    scale = lax.rsqrt(jnp.mean(total * total, axis=-1, keepdims=True) + norm_eps)
    nb[o, tp] = (total * scale * gain_ref[...]).astype(jnp.bfloat16)

    def z_copy(k):
        return rcopy(nb.at[o, tp], nb.at[o, tp], zs.at[k], zr.at[k], dev(at_o(k), h, l))

    def h_copy(k, m):
        ref = nb.at[from_o(k), tp]
        return rcopy(ref, ref, hs.at[k, m], hr.at[k, m], dev(o, at_h(m), l))

    def l_copy(k):
        ref = nb.at[from_o(k), tp]
        return rcopy(ref, ref, ls.at[k], lr.at[k], dev(o, h, other))

    def l2_copy(k, m):
        ref = nb.at[from_o(k), from_h(m) * LO + l]
        return rcopy(ref, ref, ls2.at[k, m], lr2.at[k, m], dev(o, h, other))

    def s1_copy(k):
        return rcopy(s1.at[k], r1.at[k], q1s.at[k], q1r.at[k], dev(o, h, other))

    def s2_copy(k, m):
        return rcopy(s2.at[k, m], r2.at[k, m], q2s.at[k, m], q2r.at[k, m], dev(o, at_h(m), l))

    def s3_copy(k):
        return rcopy(s3.at[k], r3.at[k], q3s.at[k], q3r.at[k], dev(from_o(k), h, l))

    for k in range(1, outer):
        z_copy(k).start()

    def forward(k):
        for m in range(1, hi):
            h_copy(k, m).start()
        l_copy(k).start()

    forward(0)

    def body(j, carry):
        @pl.when(j + 1 < outer)
        def _():
            z_copy(j + 1).wait_recv()
            forward(j + 1)

        @pl.when(j < outer)
        def _():
            for m in range(1, hi):
                h_copy(j, m).wait_recv()
                l2_copy(j, m).start()
            l_copy(j).wait_recv()
            for m in range(1, hi):
                l2_copy(j, m).wait_recv()
            x = nb[from_o(j)].reshape(tp_size * rows, depth)
            lifted = jnp.dot(x, up_ref[...], preferred_element_type=jnp.float32)
            hidden = jnp.square(jnp.maximum(lifted, 0.0)).astype(jnp.bfloat16)
            part = jnp.dot(hidden, down_ref[...], preferred_element_type=jnp.float32)
            pbuf[...] = part.reshape(tp_size, rows, depth)
            for hh in range(hi):
                s1[j, hh] = pbuf[hh * LO + other].astype(jnp.bfloat16)
            s1_copy(j).start()
            for hh in range(hi):
                acc[j, hh] = pbuf[hh * LO + l]

        @pl.when((j >= 1) & (j < outer + 1))
        def _():
            k = j - 1
            s1_copy(k).wait_recv()
            for m in range(1, hi):
                to = at_h(m)
                s2[k, m] = (acc[k, to] + r1[k, to].astype(jnp.float32)).astype(jnp.bfloat16)
                s2_copy(k, m).start()
            acc2[k] = acc[k, h] + r1[k, h].astype(jnp.float32)

        @pl.when(j >= 2)
        def _():
            k = j - 2
            v = acc2[k]
            for m in range(1, hi):
                s2_copy(k, m).wait_recv()
                v = v + r2[k, m].astype(jnp.float32)
            @pl.when(k == 0)
            def _():
                acc2[0] = v

            @pl.when(k > 0)
            def _():
                s3[k] = v.astype(jnp.bfloat16)
                s3_copy(k).start()

        return carry

    lax.fori_loop(0, outer + 2, body, 0)
    final = stream[...] + acc2[0]
    for k in range(1, outer):
        s3_copy(k).wait_recv()
        final = final + r3[k].astype(jnp.float32)
    out_ref[...] = final.astype(jnp.bfloat16)

    c5.wait_send()
    for c in c6:
        c.wait_send()
    for k in range(outer):
        if k > 0:
            z_copy(k).wait_send()
            s3_copy(k).wait_send()
        l_copy(k).wait_send()
        s1_copy(k).wait_send()
        for m in range(1, hi):
            h_copy(k, m).wait_send()
            l2_copy(k, m).wait_send()
            s2_copy(k, m).wait_send()


def mixer(sp_size, tp_size, mixed, wo, res, gain, up, down):
    rows, depth = res.shape
    hi = tp_size // LO
    f32, b16 = jnp.float32, jnp.bfloat16
    dma = pltpu.SemaphoreType.DMA
    vm = pltpu.VMEM
    O = OUTER
    return pl.pallas_call(
        functools.partial(mixer_kernel, sp_size, tp_size),
        out_shape=jax.ShapeDtypeStruct((rows, depth), b16),
        in_specs=[pl.BlockSpec(memory_space=pltpu.VMEM)] * 6,
        out_specs=pl.BlockSpec(memory_space=pltpu.VMEM),
        scratch_shapes=[
            vm((tp_size, rows, depth), f32),
            vm((rows, depth), f32),
            vm((hi, rows, depth), b16), vm((hi, rows, depth), b16),
            vm((hi, rows, depth), b16), vm((hi, rows, depth), b16),
            vm((O, tp_size, rows, depth), b16),
            vm((O, hi, rows, depth), f32),
            vm((O, hi, rows, depth), b16), vm((O, hi, rows, depth), b16),
            vm((O, hi, rows, depth), b16), vm((O, hi, rows, depth), b16),
            vm((O, rows, depth), f32),
            vm((O, rows, depth), b16), vm((O, rows, depth), b16),
            dma, dma, dma((hi,)), dma((hi,)),
            dma((O,)), dma((O,)), dma((O, hi)), dma((O, hi)),
            dma((O,)), dma((O,)), dma((O, hi)), dma((O, hi)),
            dma((O,)), dma((O,)), dma((O, hi)), dma((O, hi)),
            dma((O,)), dma((O,)),
        ],
        compiler_params=pltpu.CompilerParams(
            collective_id=0, has_side_effects=True, vmem_limit_bytes=60 * 1024 * 1024
        ),
    )(mixed, wo, res, gain.reshape(1, depth), up, down)


def regroup_weights(sp_size, up, down):
    inner = sp_size // OUTER
    inner_groups = [[o * inner + i for i in range(inner)] for o in range(OUTER)]
    down_own = lax.all_gather(down, "sp", axis=0, tiled=True, axis_index_groups=inner_groups)
    depth_part, cols = up.shape
    width = cols // OUTER
    o = lax.div(lax.axis_index("sp"), inner)
    pieces = []
    for k in range(OUTER):
        to = lax.rem(o + k, OUTER)
        piece = lax.dynamic_slice_in_dim(up, to * width, width, 1)
        if k:
            perm = [(s, (s + k * inner) % sp_size) for s in range(sp_size)]
            piece = lax.ppermute(piece, "sp", perm)
        pieces.append(piece)
    stacked = jnp.stack(pieces)
    both = lax.all_gather(stacked, "sp", axis=0, tiled=False, axis_index_groups=inner_groups)
    order = lax.rem(o - jnp.arange(OUTER) + OUTER, OUTER)
    both = jnp.take(both, order, axis=1)
    full = jnp.transpose(both, (1, 0, 2, 3)).reshape(sp_size * depth_part, width)
    return full, down_own


def on_device(
    sp_size,
    tp_size,
    query,
    forget_logits,
    written_values,
    output_gate_logits,
    forget_floor_gap,
    extra_log_decay,
    head_norm_gain,
    output_weight,
    residual,
    mixer_norm_gain,
    mixer_up_weight,
    mixer_down_weight,
):
    scaled_values, input_gate_value, value_rows, forget_log_rate = prepare_inputs(
        query, forget_logits, written_values, forget_floor_gap, extra_log_decay
    )
    row_count, local_width = query.shape
    head_count = local_width // HEAD_K
    start_state = jnp.zeros((head_count, HEAD_K, HEAD_V), jnp.float32)
    local_state, blocked = lax.scan(
        block_update,
        start_state,
        (
            to_blocks(scaled_values, HEAD_K),
            to_blocks(input_gate_value, HEAD_K),
            to_blocks(value_rows, HEAD_V),
            to_blocks(forget_log_rate, HEAD_K),
        ),
    )
    log_total = jnp.sum(forget_log_rate, axis=0).reshape(head_count, HEAD_K)
    arrived_state = carried_in(
        (log_total, local_state),
        "sp",
        chain_states,
        (jnp.zeros_like(log_total), jnp.zeros_like(local_state)),
    )
    running = jnp.cumsum(forget_log_rate, axis=0)
    reached_state = (scaled_values * jnp.exp(running)).reshape(row_count, head_count, HEAD_K)
    carried_over = jnp.einsum(
        "cja,jae->cje", reached_state, arrived_state[1], precision=highest_precision
    )
    mixed = gate_out(from_blocks(blocked) + carried_over, output_gate_logits, head_norm_gain)
    up_own, down_own = regroup_weights(sp_size, mixer_up_weight, mixer_down_weight)
    return mixer(
        sp_size, tp_size, mixed, output_weight, residual, mixer_norm_gain, up_own, down_own
    )


def solution(mesh):
    return jax.shard_map(
        functools.partial(on_device, mesh.shape["sp"], mesh.shape["tp"]),
        mesh=mesh,
        in_specs=(
            P("sp", "tp"),
            P("sp", "tp"),
            P("sp", "tp"),
            P("sp", "tp"),
            P("tp"),
            P("sp", "tp"),
            P(),
            P("tp", None),
            P(("sp", "tp"), None),
            P(),
            P("sp", "tp"),
            P(("tp", "sp"), None),
        ),
        out_specs=P(("sp", "tp"), None),
        check_vma=False,
    )
```

profile of v0, /device:TPU:0, one launch (start us, length us, event | category | flops | bytes accessed | tf_op | source)
XLA Modules:
  0.0 247.1 jit_solution(466943781068980468)
XLA Ops:
  6.5 1.2 fusion.25
  7.7 0.1 reshape.119
  7.9 0.1 reshape.120
  8.0 1.0 reshape.130
  9.1 0.2 fusion.20
  9.4 1.0 bitcast_multiply_fusion.5
  10.4 0.1 reshape.122
  10.5 22.4 %while.26 = (s32[]{:T(128)}, f32[2,128,128]{2,1,0:T(8,128)S(1)}, f32[4,2,64,128]{3,2,0,1:T(8,128)S(1)}, f32[4,2,64,128]{3,1,2,0:T(2,128)S(1)}, f32[4,2,64,128]{3...) while((s32[]{:T(128)}, f32[2,128,128]{2,1,0:T(8,128)S(1)}, ...), condition=%wide.region_2.3_spmd.clone, body=%wide.region_0.2_spmd.clone.sunk | while | flops 69382144 | bytes 10729608 | solution.py:361
  10.6 0.1 reduce_window_sum.28
  10.7 0.2 fusion.36
  11.0 0.4 convolution_add_fusion.3
  11.4 0.8 select_exponential_fusion.2
  12.3 3.5 %fusion.37 = f32[2,64,64]{1,2,0:T(8,128)S(1)} fusion(f32[2,64,64,128]{3,2,1,0:T(8,128)S(1)} %select_exponential_fusion.2, f32[2,128,64]{1,2,0:T(8,128)S(1)} %bitcast.113, f32[2,128,64]{1,2,0:T(8,128)S(1)} %bitcast.114), kind=kLoop, calls=%fused_computation.4.clone.1 | loop fusion | flops 3137536 | bytes 4358144 | tf_op jit(solution)/shard_map/while/body/eval_jaxpr/htk,hsk,htsk->hts/dot_general | solution.py:45
  15.8 0.3 fusion.38
  16.3 0.2 fusion.36
  16.6 0.4 convolution_add_fusion.3
  17.0 0.8 select_exponential_fusion.2
  17.9 3.5 %fusion.37 = f32[2,64,64]{1,2,0:T(8,128)S(1)} fusion(f32[2,64,64,128]{3,2,1,0:T(8,128)S(1)} %select_exponential_fusion.2, f32[2,128,64]{1,2,0:T(8,128)S(1)} %bitcast.113, f32[2,128,64]{1,2,0:T(8,128)S(1)} %bitcast.114), kind=kLoop, calls=%fused_computation.4.clone.1 | loop fusion | flops 3137536 | bytes 4358144 | tf_op jit(solution)/shard_map/while/body/eval_jaxpr/htk,hsk,htsk->hts/dot_general | solution.py:45
  21.5 0.3 fusion.38
  21.9 0.2 fusion.36
  22.2 0.4 convolution_add_fusion.3
  22.6 0.8 select_exponential_fusion.2
  23.5 3.5 %fusion.37 = f32[2,64,64]{1,2,0:T(8,128)S(1)} fusion(f32[2,64,64,128]{3,2,1,0:T(8,128)S(1)} %select_exponential_fusion.2, f32[2,128,64]{1,2,0:T(8,128)S(1)} %bitcast.113, f32[2,128,64]{1,2,0:T(8,128)S(1)} %bitcast.114), kind=kLoop, calls=%fused_computation.4.clone.1 | loop fusion | flops 3137536 | bytes 4358144 | tf_op jit(solution)/shard_map/while/body/eval_jaxpr/htk,hsk,htsk->hts/dot_general | solution.py:45
  27.1 0.3 fusion.38
  27.5 0.2 fusion.36
  27.8 0.4 convolution_add_fusion.3
  28.2 0.8 select_exponential_fusion.2
  29.1 3.5 %fusion.37 = f32[2,64,64]{1,2,0:T(8,128)S(1)} fusion(f32[2,64,64,128]{3,2,1,0:T(8,128)S(1)} %select_exponential_fusion.2, f32[2,128,64]{1,2,0:T(8,128)S(1)} %bitcast.113, f32[2,128,64]{1,2,0:T(8,128)S(1)} %bitcast.114), kind=kLoop, calls=%fused_computation.4.clone.1 | loop fusion | flops 3137536 | bytes 4358144 | tf_op jit(solution)/shard_map/while/body/eval_jaxpr/htk,hsk,htsk->hts/dot_general | solution.py:45
  32.7 0.3 fusion.38
  33.0 0.6 copy-done
  33.8 0.1 dynamic-slice_bitcast_fusion
  33.9 5.1 %collective-permute-start.2 = (bf16[256,512]{1,0:T(8,128)(2,1)S(1)}, bf16[256,512]{1,0:T(8,128)(2,1)S(1)}, u32[]{:S(2)}, u32[]{:S(2)}) collective-permute-start(bf16[256,512]{1,0:T(8,128)(2,1)S(1)} %get-tuple-element.167), channel_id=1, source_target_pairs={{0,24},{4,28},{8,0},{12,4},{16,8},{20,12},{24,16},{28,20},{1,25},{... | collective-permute-start | bytes 786440 | tf_op jit(solution)/shard_map/ppermute | solution.py:329
  39.0 1.0 collective-permute-start
  40.0 6.4 %collective-permute-done.2 = bf16[256,512]{1,0:T(8,128)(2,1)S(1)} collective-permute-done((bf16[256,512]{1,0:T(8,128)(2,1)S(1)}, bf16[256,512]{1,0:T(8,128)(2,1)S(1)}, u32[]{:S(2)}, u32[]{:S(2)}) %collective-permute-start.2) | collective-permute-done | bytes 262176 | tf_op jit(solution)/shard_map/ppermute | solution.py:329
  46.5 19.1 %collective-permute-done.1 = bf16[256,512]{1,0:T(8,128)(2,1)S(1)} collective-permute-done((bf16[256,512]{1,0:T(8,128)(2,1)S(1)}, bf16[256,512]{1,0:T(8,128)(2,1)S(1)}, u32[]{:S(2)}, u32[]{:S(2)}) %collective-permute-start.1) | collective-permute-done | bytes 262176 | tf_op jit(solution)/shard_map/ppermute | solution.py:329
  65.6 1.1 pad_maximum_fusion
  66.7 0.7 all-gather.6.cloned.1.call-update
  67.6 0.1 copy.59
  67.7 0.1 copy.58
  67.8 18.4 %all_gather.18 = f32[8,2,128]{2,1,0:T(2,128)S(1)} all-gather(f32[1,2,128]{2,1,0:T(2,128)S(1)} %bitcast.135), channel_id=1, replica_groups=mesh['sp'=8,'tp'=4] {'sp'}, dimensions={0}, use_global_device_ids=true | all-gather | bytes 9216 | tf_op jit(solution)/shard_map/all_gather | solution.py:21
  86.2 0.4 multiply_reduce_fusion
  86.8 0.8 copy.69.mixed_ref
  87.6 31.8 %all-gather.10.cloned.1.call-done = bf16[8,256,512]{2,1,0:T(8,128)(2,1)} async-done(((bf16[4,256,512]{2,1,0:T(8,128)(2,1)}), bf16[8,256,512]{2,1,0:T(8,128)(2,1)}) %all-gather.10.cloned.1.call-update) | async-done | bytes 2097168 | tf_op jit(solution)/shard_map/all_gather | solution.py:332
  119.4 2.3 gather_fusion
  121.6 1.6 broadcast_select_fusion
  123.2 30.8 %all-gather.6.cloned.1.call-done.down_ref = bf16[512,2048]{1,0:T(8,128)(2,1)} async-done(((bf16[256,2048]{1,0:T(8,128)(2,1)}), bf16[512,2048]{1,0:T(8,128)(2,1)}) %all-gather.6.cloned.1.call-update) | async-done | bytes 2097168 | tf_op jit(solution)/shard_map/all_gather | solution.py:319
  154.0 84.9 %shard_map.118 = bf16[64,2048]{1,0:T(8,128)(2,1)} custom-call(bf16[256,256]{1,0:T(8,128)(2,1)} %copy.69.mixed_ref, bf16[256,2048]{1,0:T(8,128)(2,1)} %wo_ref.1, bf16[64,2048]{1,0:T(8,128)(2,1)} %res_ref.1, f32[1,2048]{1,0:T(1,128)} %bitcast.134, bf16[2048,512]{1,0:T(8,128)(2,1)} %bitcast.112, bf16[512,2048]{1,0:T(8,128)(2,1)} %all-gather.6.cloned.1.call-done.down_ref), custom_call_target="tpu_custom_call" | custom-call | tf_op jit(solution)/shard_map/pallas_call | solution.py:288
  238.9 1.7 copy.140
  (66 shorter events, 1.1 us)
Async XLA Ops:
  6.5 79.7 %all-gather.8.cloned.1.call-start = ((), (), s32[]{:S(2)}) async-start(), calls=%async_computation.1 | async-start | bytes 1179648 | tf_op jit(solution)/shard_map/all_gather | solution.py:21
  10.5 23.2 %copy-start.1 = (bf16[256,2048]{1,0:T(8,128)(2,1)S(1)}, bf16[256,2048]{1,0:T(8,128)(2,1)}, u32[]{:S(2)}) copy-start(bf16[256,2048]{1,0:T(8,128)(2,1)} %param.26) | copy-start | bytes 3145732
  33.0 0.7 copy-start
  33.0 34.5 %copy-start.2 = (bf16[256,256]{1,0:T(8,128)(2,1)S(1)}, bf16[256,256]{1,0:T(8,128)(2,1)}, u32[]{:S(2)}) copy-start(bf16[256,256]{1,0:T(8,128)(2,1)} %param.19) | copy-start | bytes 393220
  33.7 85.7 %all-gather.10.cloned.1.call-start = ((), (), s32[]{:S(2)}) async-start(), calls=%async_computation.2 | async-start | bytes 3145728 | tf_op jit(solution)/shard_map/all_gather | solution.py:332
  33.9 12.6 %collective-permute-start.2 = (bf16[256,512]{1,0:T(8,128)(2,1)S(1)}, bf16[256,512]{1,0:T(8,128)(2,1)S(1)}, u32[]{:S(2)}, u32[]{:S(2)}) collective-permute-start(bf16[256,512]{1,0:T(8,128)(2,1)S(1)} %get-tuple-element.167), channel_id=1, source_target_pairs={{0,24},{4,28},{8,0},{12,4},{16,8},{20,12},{24,16},{28,20},{1,25},{... | collective-permute-start | bytes 786440 | tf_op jit(solution)/shard_map/ppermute | solution.py:329
  39.0 26.5 %collective-permute-start.1 = (bf16[256,512]{1,0:T(8,128)(2,1)S(1)}, bf16[256,512]{1,0:T(8,128)(2,1)S(1)}, u32[]{:S(2)}, u32[]{:S(2)}) collective-permute-start(bf16[256,512]{1,0:T(8,128)(2,1)S(1)} %get-tuple-element.168), channel_id=1, source_target_pairs={{0,16},{4,20},{8,24},{12,28},{16,0},{20,4},{24,8},{28,12},{1,17},{... | collective-permute-start | bytes 786440 | tf_op jit(solution)/shard_map/ppermute | solution.py:329
  39.0 26.5 %collective-permute-start = (bf16[256,512]{1,0:T(8,128)(2,1)S(1)}, bf16[256,512]{1,0:T(8,128)(2,1)S(1)}, u32[]{:S(2)}, u32[]{:S(2)}) collective-permute-start(bf16[256,512]{1,0:T(8,128)(2,1)S(1)} %get-tuple-element.166), channel_id=1, source_target_pairs={{0,8},{4,12},{8,16},{12,20},{16,24},{20,28},{24,0},{28,4},{1,9},{5... | collective-permute-start | bytes 786440 | tf_op jit(solution)/shard_map/ppermute | solution.py:329
  65.6 21.1 %copy-start.3 = (f32[128]{0:T(128)S(1)}, f32[128]{0:T(128)}, u32[]{:S(2)}) copy-start(f32[128]{0:T(128)} %param.22) | copy-start | bytes 1540
  66.7 87.3 %all-gather.6.cloned.1.call-start = ((), (), s32[]{:S(2)}) async-start(), calls=%async_computation | async-start | bytes 3145728 | tf_op jit(solution)/shard_map/all_gather | solution.py:319
Sparse Core Ops, SparseCore 0:
  33.8 52.3 all-gather.7
  87.7 31.6 all-gather.9
  120.9 33.0 all-gather.5
where the time goes:
time: 247 us
  waiting for transfers between devices  88.8 us (36%)
  Pallas kernels  84.9 us (34%)
  other arithmetic  23.3 us (9%)
  blocking collectives  18.4 us (7%)
  between operations  13.4 us (5%)
  local copies, waits for them, and re-layouts  7.46 us (3%)
  starting transfers between devices  6.23 us (3%)
  matrix products  4.22 us (2%)
    pallas_call x1, Pallas kernels, mixer(): pl.pallas_call(functools.partial(mixer_kernel, sp_size, tp_size), out_sha...  84.9 us
    all_gather x1, waiting for transfers between devices, regroup_weights(): lax.all_gather(stacked, 'sp', axis=0, tiled=False, axis_index_groups=inne...  31.8 us
    all_gather x1, waiting for transfers between devices, regroup_weights(): lax.all_gather(down, 'sp', axis=0, tiled=True, axis_index_groups=inner_gr...  30.8 us
    ppermute x3, waiting for transfers between devices, regroup_weights(): piece = lax.ppermute(piece, 'sp', perm)  25.5 us
    all_gather x1, blocking collectives, carried_in(): gathered = jax.tree.map(lambda a: lax.all_gather(a, axis), part)  18.4 us
    dot_general x4, other arithmetic, block_update(): jnp.einsum('htk,hsk,htsk->hts', query_rows_block, gate_rows_block, decay_...  14.2 us
    ppermute x3, starting transfers between devices, regroup_weights(): piece = lax.ppermute(piece, 'sp', perm)  6.14 us
  transfers between devices with their start and end apart: 6, of which 4 were waited for; matrix products, arithmetic and copies ran while one was open for 3% of the time, Pallas kernels for 0%

commit v1 on v0

v1 whole, which is shorter than its diff:
```python
import functools

import jax
import jax.numpy as jnp
from jax import lax
from jax.experimental import pallas as pl
from jax.experimental.pallas import tpu as pltpu
from jax.sharding import PartitionSpec as P

HEAD_K = 128
HEAD_V = 128
CHUNK = 128
OUTER = 4
LO = 2
MESH = pl.DeviceIdType.MESH
norm_eps = 1e-06


def doubling(n):
    d, out = 1, []
    while d < n:
        out.append(d)
        d *= 2
    return out


def hops(n):
    return [s * k for k in range(1, n) for s in (1, -1)]


def by_distance(n):
    return [sorted(range(n), key=lambda c: (abs(c - o), c)) for o in range(n)]


def dot_t(a, b):
    return lax.dot_general(a, b, (((1,), (1,)), ((), ())), preferred_element_type=jnp.float32)


def dot_0(a, b):
    return lax.dot_general(a, b, (((0,), (0,)), ((), ())), preferred_element_type=jnp.float32)


def dot(a, b):
    return jnp.dot(a, b, preferred_element_type=jnp.float32)


def layer_kernel(
    sp_size, tp_size, up_pieces, down_pieces,
    q_hbm, f_hbm, v_hbm, g_hbm, gap_hbm, ex_hbm, hg_hbm, wo_hbm, res_hbm, mg_hbm, up_hbm, dn_hbm,
    out_ref,
    qb, fb, vb, gb, exb, gapb, hgb, mgb, resb,
    cumb, gateb, recb, qcb, own, ownl, exc, excl, ss, sl, rs_, rl,
    mixb, mx, wob, upb, dnb,
    stream, nb, pbuf, acc, s1, r1, s2, r2, acc2, s3, r3,
    ldsem, sts, str_, lts, ltr, mxs, mxr, wos, wor, wfs, wfr, us, ur, fs, fr, dsn, dr,
    zs, zr, hs, hr, ls, lr, ls2, lr2, q1s, q1r, q2s, q2r, q3s, q3r,
):
    outer, inner, hi = OUTER, sp_size // OUTER, tp_size // LO
    sp, tp = lax.axis_index("sp"), lax.axis_index("tp")
    o, i = lax.div(sp, inner), lax.rem(sp, inner)
    h, l = lax.div(tp, LO), lax.rem(tp, LO)
    other = 1 - l
    rows, depth = res_hbm.shape
    length, local_width = q_hbm.shape
    heads = local_width // HEAD_K
    depth_part, cols = up_hbm.shape
    width = cols // outer
    down_rows = dn_hbm.shape[0]
    f32, b16 = jnp.float32, jnp.bfloat16
    steps = doubling(sp_size)

    def dev(ss_, tt):
        return (ss_, tt)

    def at_h(m):
        return lax.rem(h + m, hi)

    def from_h(m):
        return lax.rem(h - m + hi, hi)

    def at_i(m):
        return lax.rem(i + m, inner)

    def from_i(m):
        return lax.rem(i - m + inner, inner)

    def at_t(m):
        return lax.rem(tp + m, tp_size)

    def from_t(m):
        return lax.rem(tp - m + tp_size, tp_size)

    def rcopy(src, dst, ssem, rsem, device):
        return pltpu.make_async_remote_copy(
            src_ref=src, dst_ref=dst, send_sem=ssem, recv_sem=rsem,
            device_id=device, device_id_type=MESH,
        )

    loads = [
        pltpu.make_async_copy(src, dst, ldsem.at[n])
        for n, (src, dst) in enumerate(
            [
                (f_hbm, fb), (ex_hbm, exb), (gap_hbm, gapb), (v_hbm, vb), (q_hbm, qb), (g_hbm, gb),
                (hg_hbm, hgb), (mg_hbm, mgb), (res_hbm, resb),
                (wo_hbm, wob.at[tp]),
                (up_hbm.at[:, pl.ds(pl.multiple_of(o * width, width), width)], upb.at[sp]),
                (dn_hbm, dnb.at[i]),
            ]
        )
    ]
    for c in loads:
        c.start()

    barrier = pltpu.get_barrier_semaphore()
    peers = [dev(lax.rem(o + k, outer) * inner + i, tp) for k in range(1, outer)]
    peers += [dev(o * inner + at_i(m), tp) for m in range(1, inner)]
    peers += [dev(sp, at_t(m)) for m in range(1, tp_size)]
    for d in steps:
        peers += [dev(lax.rem(sp + d, sp_size), tp), dev(lax.rem(sp - d + sp_size, sp_size), tp)]
    for peer in peers:
        pl.semaphore_signal(barrier, inc=1, device_id=peer, device_id_type=MESH)
    pl.semaphore_wait(barrier, len(peers))

    up_rows = depth_part // up_pieces
    dn_rows = down_rows // down_pieces

    def up_cols(to, p):
        return up_hbm.at[
            pl.ds(p * up_rows, up_rows), pl.ds(pl.multiple_of(to * width, width), width)
        ]

    def up_place(source, p):
        return upb.at[source, pl.ds(p * up_rows, up_rows)]

    def up_send(to, p):
        return rcopy(
            up_cols(to, p), up_place(sp, p), us.at[to, p], ur.at[o, p], dev(to * inner + i, tp)
        )

    def up_recv(source, p):
        place = up_place(source * inner + i, p)
        return rcopy(place, place, us.at[source, p], ur.at[source, p], dev(source * inner + i, tp))

    def fw_send(source, p, m, src):
        return rcopy(
            src, up_place(source * inner + i, p), fs.at[source, p, m], fr.at[source, p, m],
            dev(o * inner + at_i(m), tp),
        )

    def fw_recv(source, p, m):
        place = up_place(source * inner + from_i(m), p)
        return rcopy(
            place, place, fs.at[source, p, m], fr.at[source, p, m], dev(o * inner + from_i(m), tp)
        )

    def dn_send(p, m):
        part = pl.ds(p * dn_rows, dn_rows)
        return rcopy(
            dn_hbm.at[part], dnb.at[i, part], dsn.at[p, m], dr.at[p, m],
            dev(o * inner + at_i(m), tp),
        )

    def dn_recv(p, m):
        place = dnb.at[from_i(m), pl.ds(p * dn_rows, dn_rows)]
        return rcopy(place, place, dsn.at[p, m], dr.at[p, m], dev(o * inner + from_i(m), tp))

    def inside(k):
        return (o + k >= 0) & (o + k < outer)

    def up_issue(items):
        for k, p in items:
            @pl.when(inside(k))
            def _():
                up_send(o + k, p).start()

    def own_issue(p):
        for m in range(1, inner):
            fw_send(o, p, m, up_cols(o, p)).start()

    def dn_issue(p):
        for m in range(1, inner):
            dn_send(p, m).start()

    def fw_issue(items):
        for k, p in items:
            @pl.when(inside(k))
            def _():
                up_recv(o + k, p).wait_recv()
                for m in range(1, inner):
                    fw_send(o + k, p, m, up_place((o + k) * inner + i, p)).start()

    up_list = [(k, p) for k in hops(outer) for p in range(up_pieces)]
    near = [(k, p) for k, p in up_list if abs(k) == 1]
    groups = [[(k, p) for k, p in near if p == 0], [(k, p) for k, p in near if p > 0]]
    far = [(k, p) for k, p in up_list if abs(k) > 1]
    groups += [[(k, p) for k, p in far if abs(k) == 2 and p == 0]]
    rest = [it for it in far if it not in groups[2]]

    def wo_send_l():
        return rcopy(wo_hbm, wob.at[tp], wos.at[0], wor.at[0], dev(sp, h * LO + other))

    def wo_send_h(m):
        return rcopy(wo_hbm, wob.at[tp], wos.at[m], wor.at[m], dev(sp, at_h(m) * LO + l))

    def wo_recv_h(m):
        place = wob.at[from_h(m) * LO + l]
        return rcopy(place, place, wos.at[m], wor.at[m], dev(sp, from_h(m) * LO + l))

    def wo_fw(m):
        place = wob.at[from_h(m) * LO + l]
        return rcopy(place, place, wfs.at[m], wfr.at[m], dev(sp, h * LO + other))

    wo_send_l().start()
    for m in range(1, hi):
        wo_send_h(m).start()
    own_issue(0)
    up_issue(groups[0])

    for c in loads[:4]:
        c.wait()
    gate = gapb[...] / (1.0 + jnp.exp(fb[...].astype(f32)))
    gateb[...] = gate
    log_rate = jnp.log(1.0 - gate) + exb[...]
    top = log_rate.astype(b16)
    left = log_rate - top.astype(f32)
    middle = left.astype(b16)
    low = (left - middle.astype(f32)).astype(b16)
    causal = lax.broadcasted_iota(jnp.int32, (length, length), 0) >= lax.broadcasted_iota(
        jnp.int32, (length, length), 1
    )
    ones = jnp.where(causal, 1.0, 0.0).astype(b16)
    cum = dot(ones, top) + (dot(ones, middle) + dot(ones, low))
    cumb[...] = cum
    total_log = cum[length - 1 : length, :]
    written = (gate * jnp.exp(total_log - cum)).astype(b16)
    exc[...] = jnp.zeros_like(exc)
    excl[...] = jnp.zeros_like(excl)
    sl[...] = jnp.zeros_like(sl)
    for n in range(heads):
        at = slice(n * HEAD_K, (n + 1) * HEAD_K)
        state = dot_0(vb[:, at], written[:, at])
        own[n] = state
        ss[0, n] = state.astype(b16)
        ownl[n : n + 1, :] = total_log[:, at]
        sl[0, n : n + 1, :] = total_log[:, at]

    def st_send(n):
        return rcopy(ss.at[n], rs_.at[n], sts.at[n], str_.at[n], dev(sp + steps[n], tp))

    def lt_send(n):
        return rcopy(sl.at[n], rl.at[n], lts.at[n], ltr.at[n], dev(sp + steps[n], tp))

    def step_send(n):
        @pl.when(sp + steps[n] < sp_size)
        def _():
            lt_send(n).start()
            st_send(n).start()

    def step_recv(n):
        @pl.when(sp >= steps[n])
        def _():
            lt_send(n).wait_recv()
            st_send(n).wait_recv()
            for k in range(heads):
                exc[k] = exc[k] + jnp.exp(excl[k : k + 1, :]) * rs_[n, k].astype(f32)
                excl[k : k + 1, :] = excl[k : k + 1, :] + rl[n, k : k + 1, :]

    def step_pack(n):
        for k in range(heads):
            ss[n, k] = (own[k] + jnp.exp(ownl[k : k + 1, :]) * exc[k]).astype(b16)
            sl[n, k : k + 1, :] = ownl[k : k + 1, :] + excl[k : k + 1, :]

    step_send(0)
    up_issue(groups[1])
    for p in range(1, up_pieces):
        own_issue(p)
    for p in range(down_pieces):
        dn_issue(p)

    loads[4].wait()
    scaled = qb[...].astype(f32) * HEAD_K ** (-0.5)
    qcb[...] = (scaled * jnp.exp(cum)).astype(b16)
    blocks = length // CHUNK
    tri = causal[:CHUNK, :CHUNK]
    for a in range(blocks):
        r = slice(a * CHUNK, (a + 1) * CHUNK)
        c_a, g_a, q_a = cum[r], gate[r], scaled[r]
        end = cum[(a + 1) * CHUNK - 1 : (a + 1) * CHUNK, :]
        base = cum[a * CHUNK - 1 : a * CHUNK, :] if a else jnp.zeros_like(end)
        mid = 0.5 * (end + base)
        q_d = (q_a * jnp.exp(c_a - mid)).astype(b16)
        k_d = (g_a * jnp.exp(mid - c_a)).astype(b16)
        if a:
            before = slice(0, a * CHUNK)
            q_o = (q_a * jnp.exp(c_a - base)).astype(b16)
            k_o = (gate[before] * jnp.exp(base - cum[before])).astype(b16)
        for n in range(heads):
            at = slice(n * HEAD_K, (n + 1) * HEAD_K)
            score = jnp.where(tri, dot_t(q_d[:, at], k_d[:, at]), 0.0).astype(b16)
            got = dot(score, vb[r, at])
            if a:
                score = dot_t(q_o[:, at], k_o[:, at]).astype(b16)
                got = got + dot(score, vb[before, at])
            recb[r, at] = got

    for n in range(len(steps)):
        step_recv(n)
        if n + 1 < len(steps):
            step_pack(n + 1)
            step_send(n + 1)
            if n == 0:
                up_issue(groups[2])
            if n + 2 == len(steps):
                up_issue(rest)
    if len(steps) < 2:
        up_issue(groups[2])
        up_issue(rest)

    loads[5].wait()
    loads[6].wait()
    for n in range(heads):
        at = slice(n * HEAD_K, (n + 1) * HEAD_K)
        rec = recb[:, at] + dot_t(qcb[:, at], exc[n].astype(b16))
        logits = gb[:, at].astype(f32)
        normal = rec * lax.rsqrt(jnp.mean(rec * rec, axis=-1, keepdims=True) + norm_eps)
        mixed = (normal * hgb[...] * (logits / (1.0 + jnp.exp(-logits)))).astype(b16)
        mixb[:, :, at] = mixed.reshape(tp_size, rows, HEAD_V)

    def mx_send(m):
        return rcopy(mixb.at[at_t(m)], mx.at[tp], mxs.at[m], mxr.at[m], dev(sp, at_t(m)))

    def mx_recv(m):
        place = mx.at[from_t(m)]
        return rcopy(place, place, mxs.at[m], mxr.at[m], dev(sp, from_t(m)))

    for m in range(1, tp_size):
        mx_send(m).start()
    mx[tp] = mixb[tp]
    fw_issue(near)

    for m in range(1, hi):
        wo_recv_h(m).wait_recv()
        wo_fw(m).start()
    for m in range(1, tp_size):
        mx_recv(m).wait_recv()
    for c in loads[7:10]:
        c.wait()
    wo_send_l().wait_recv()
    total = resb[...].astype(f32)
    for ll in range(LO):
        t = h * LO + ll
        total = total + dot(mx[t], wob[t])
    for m in range(1, hi):
        t = from_h(m) * LO + l
        total = total + dot(mx[t], wob[t])
    for m in range(1, hi):
        wo_fw(m).wait_recv()
        t = from_h(m) * LO + other
        total = total + dot(mx[t], wob[t])
    stream[...] = total
    scale = lax.rsqrt(jnp.mean(total * total, axis=-1, keepdims=True) + norm_eps)
    nb[o, tp] = (total * scale * mgb[...]).astype(b16)

    table = by_distance(outer)

    def chunk_at(p):
        c = 0
        for oo in range(outer):
            for pp in range(outer):
                c = jnp.where((o == oo) & (p == pp), table[oo][pp], c)
        return c

    def z_copy(c, to):
        ref = nb.at[c, tp]
        return rcopy(ref, ref, zs.at[c, to], zr.at[c], dev(to * inner + i, tp))

    def h_copy(c, m):
        ref = nb.at[c, tp]
        return rcopy(ref, ref, hs.at[c, m], hr.at[c, m], dev(sp, at_h(m) * LO + l))

    def l_copy(c):
        ref = nb.at[c, tp]
        return rcopy(ref, ref, ls.at[c], lr.at[c], dev(sp, h * LO + other))

    def l2_copy(c, m):
        ref = nb.at[c, from_h(m) * LO + l]
        return rcopy(ref, ref, ls2.at[c, m], lr2.at[c, m], dev(sp, h * LO + other))

    def pass_up(c):
        @pl.when((c <= o) & (o + 1 < outer))
        def _():
            z_copy(c, o + 1).start()

        @pl.when((c >= o) & (o > 0))
        def _():
            z_copy(c, o - 1).start()

    def spread(c):
        for m in range(1, hi):
            h_copy(c, m).start()
        l_copy(c).start()

    def gather(c):
        for m in range(1, hi):
            h_copy(c, m).wait_recv()
            l2_copy(c, m).start()

    pass_up(o)
    spread(o)
    fw_issue(groups[2] + rest)

    def ag_body(p, carry):
        c = chunk_at(p)
        z_copy(c, o).wait_recv()
        pass_up(c)
        spread(c)
        gather(chunk_at(p - 1))
        return carry

    lax.fori_loop(1, outer, ag_body, 0)
    gather(chunk_at(outer - 1))

    for c in loads[10:]:
        c.wait()
    for k in [0] + hops(outer):
        @pl.when(inside(k))
        def _():
            for p in range(up_pieces):
                for m in range(1, inner):
                    fw_recv(o + k, p, m).wait_recv()
    for p in range(down_pieces):
        for m in range(1, inner):
            dn_recv(p, m).wait_recv()

    def s1_copy(k):
        return rcopy(s1.at[k], r1.at[k], q1s.at[k], q1r.at[k], dev(sp, h * LO + other))

    def s2_copy(k, m):
        return rcopy(s2.at[k, m], r2.at[k, m], q2s.at[k, m], q2r.at[k, m], dev(sp, at_h(m) * LO + l))

    def s3_copy(c):
        return rcopy(s3.at[c], r3.at[o], q3s.at[c], q3r.at[o], dev(c * inner + i, tp))

    def s3_recv(c):
        return rcopy(r3.at[c], r3.at[c], q3s.at[c], q3r.at[c], dev(c * inner + i, tp))

    def turn(j):
        return chunk_at(outer - 1 - j)

    def body(j, carry):
        @pl.when(j < outer)
        def _():
            c = turn(j)
            l_copy(c).wait_recv()
            for m in range(1, hi):
                l2_copy(c, m).wait_recv()
            x = nb[c].reshape(tp_size * rows, depth)
            lifted = dot(x, upb[...].reshape(depth, width))
            hidden = jnp.square(jnp.maximum(lifted, 0.0)).astype(b16)
            part = dot(hidden, dnb[...].reshape(width, depth))
            pbuf[...] = part.reshape(tp_size, rows, depth)
            for hh in range(hi):
                s1[j, hh] = pbuf[hh * LO + other].astype(b16)
            s1_copy(j).start()
            for hh in range(hi):
                acc[j, hh] = pbuf[hh * LO + l]

        @pl.when((j >= 1) & (j < outer + 1))
        def _():
            k = j - 1
            s1_copy(k).wait_recv()
            for m in range(1, hi):
                to = at_h(m)
                s2[k, m] = (acc[k, to] + r1[k, to].astype(f32)).astype(b16)
                s2_copy(k, m).start()
            acc2[k] = acc[k, h] + r1[k, h].astype(f32)

        @pl.when(j >= 2)
        def _():
            k = j - 2
            v = acc2[k]
            for m in range(1, hi):
                s2_copy(k, m).wait_recv()
                v = v + r2[k, m].astype(f32)

            @pl.when(k < outer - 1)
            def _():
                c = turn(k)
                s3[c] = v.astype(b16)
                s3_copy(c).start()

            @pl.when(k == outer - 1)
            def _():
                stream[...] = stream[...] + v

        return carry

    lax.fori_loop(0, outer + 2, body, 0)
    final = stream[...]
    for k in range(1, outer):
        c = chunk_at(k)
        s3_recv(c).wait_recv()
        final = final + r3[c].astype(f32)
    out_ref[...] = final.astype(b16)

    wo_send_l().wait_send()
    for m in range(1, hi):
        wo_send_h(m).wait_send()
        wo_fw(m).wait_send()
    for m in range(1, tp_size):
        mx_send(m).wait_send()
    for n in range(len(steps)):
        @pl.when(sp + steps[n] < sp_size)
        def _():
            lt_send(n).wait_send()
            st_send(n).wait_send()
    for k, p in up_list:
        @pl.when(inside(k))
        def _():
            up_send(o + k, p).wait_send()
            for m in range(1, inner):
                fw_send(o + k, p, m, up_place((o + k) * inner + i, p)).wait_send()
    for m in range(1, inner):
        for p in range(up_pieces):
            fw_send(o, p, m, up_cols(o, p)).wait_send()
        for p in range(down_pieces):
            dn_send(p, m).wait_send()
    for c in range(outer):
        @pl.when((c <= o) & (o + 1 < outer))
        def _():
            z_copy(c, o + 1).wait_send()

        @pl.when((c >= o) & (o > 0))
        def _():
            z_copy(c, o - 1).wait_send()

        @pl.when(c != o)
        def _():
            s3_copy(c).wait_send()

        l_copy(c).wait_send()
        s1_copy(c).wait_send()
        for m in range(1, hi):
            h_copy(c, m).wait_send()
            l2_copy(c, m).wait_send()
            s2_copy(c, m).wait_send()


def on_device(
    sp_size, tp_size, query, forget_logits, written_values, output_gate_logits, forget_floor_gap,
    extra_log_decay, head_norm_gain, output_weight, residual, mixer_norm_gain, mixer_up_weight,
    mixer_down_weight,
):
    rows, depth = residual.shape
    length, local_width = query.shape
    heads = local_width // HEAD_K
    depth_part, cols = mixer_up_weight.shape
    down_rows = mixer_down_weight.shape[0]
    inner, hi = sp_size // OUTER, tp_size // LO
    width = cols // OUTER
    up_pieces = max(1, min(2, depth_part // 128))
    down_pieces = max(1, min(4, down_rows // 64))
    steps = len(doubling(sp_size))
    f32, b16 = jnp.float32, jnp.bfloat16
    dma = pltpu.SemaphoreType.DMA
    vm = pltpu.VMEM
    O = OUTER
    lrows = 8 * ((heads + 7) // 8)
    return pl.pallas_call(
        functools.partial(layer_kernel, sp_size, tp_size, up_pieces, down_pieces),
        out_shape=jax.ShapeDtypeStruct((rows, depth), b16),
        in_specs=[pl.BlockSpec(memory_space=pltpu.HBM)] * 12,
        out_specs=pl.BlockSpec(memory_space=pltpu.VMEM),
        scratch_shapes=[
            vm((length, local_width), b16), vm((length, local_width), b16),
            vm((length, local_width), b16), vm((length, local_width), b16),
            vm((length, local_width), f32),
            vm((1, local_width), f32), vm((1, HEAD_V), f32), vm((1, depth), f32),
            vm((rows, depth), b16),
            vm((length, local_width), f32), vm((length, local_width), f32),
            vm((length, local_width), f32), vm((length, local_width), b16),
            vm((heads, HEAD_V, HEAD_K), f32), vm((lrows, HEAD_K), f32),
            vm((heads, HEAD_V, HEAD_K), f32), vm((lrows, HEAD_K), f32),
            vm((steps, heads, HEAD_V, HEAD_K), b16), vm((steps, lrows, HEAD_K), f32),
            vm((steps, heads, HEAD_V, HEAD_K), b16), vm((steps, lrows, HEAD_K), f32),
            vm((tp_size, rows, local_width), b16), vm((tp_size, rows, local_width), b16),
            vm((tp_size, local_width, depth), b16),
            vm((sp_size, depth_part, width), b16),
            vm((inner, down_rows, depth), b16),
            vm((rows, depth), f32),
            vm((O, tp_size, rows, depth), b16),
            vm((tp_size, rows, depth), f32),
            vm((O, hi, rows, depth), f32),
            vm((O, hi, rows, depth), b16), vm((O, hi, rows, depth), b16),
            vm((O, hi, rows, depth), b16), vm((O, hi, rows, depth), b16),
            vm((O, rows, depth), f32),
            vm((O, rows, depth), b16), vm((O, rows, depth), b16),
            dma((12,)),
            dma((steps,)), dma((steps,)), dma((steps,)), dma((steps,)),
            dma((tp_size,)), dma((tp_size,)),
            dma((hi,)), dma((hi,)), dma((hi,)), dma((hi,)),
            dma((O, up_pieces)), dma((O, up_pieces)),
            dma((O, up_pieces, inner)), dma((O, up_pieces, inner)),
            dma((down_pieces, inner)), dma((down_pieces, inner)),
            dma((O, O)), dma((O,)),
            dma((O, hi)), dma((O, hi)),
            dma((O,)), dma((O,)), dma((O, hi)), dma((O, hi)),
            dma((O,)), dma((O,)), dma((O, hi)), dma((O, hi)),
            dma((O,)), dma((O,)),
        ],
        compiler_params=pltpu.CompilerParams(
            collective_id=0, has_side_effects=True, vmem_limit_bytes=60 * 1024 * 1024
        ),
    )(
        query, forget_logits, written_values, output_gate_logits, forget_floor_gap.reshape(1, -1),
        extra_log_decay, head_norm_gain.reshape(1, -1), output_weight, residual,
        mixer_norm_gain.reshape(1, -1), mixer_up_weight, mixer_down_weight,
    )


def solution(mesh):
    return jax.shard_map(
        functools.partial(on_device, mesh.shape["sp"], mesh.shape["tp"]),
        mesh=mesh,
        in_specs=(
            P("sp", "tp"),
            P("sp", "tp"),
            P("sp", "tp"),
            P("sp", "tp"),
            P("tp"),
            P("sp", "tp"),
            P(),
            P("tp", None),
            P(("sp", "tp"), None),
            P(),
            P("sp", "tp"),
            P(("tp", "sp"), None),
        ),
        out_specs=P(("sp", "tp"), None),
        check_vma=False,
    )
```

time: 247 us -> 100 us (0.40)
  waiting for transfers between devices: 88.8 us -> 0 us
  other arithmetic: 23.3 us -> 0 us
  blocking collectives: 18.4 us -> 0 us
  between operations: 13.4 us -> 0.01 us
  Pallas kernels: 84.9 us -> 98.1 us
  starting transfers between devices: 6.23 us -> 0 us
  local copies, waits for them, and re-layouts: 7.46 us -> 1.67 us
  matrix products: 4.22 us -> 0 us
    all_gather x3 -> x0, waiting for transfers between devices: 62.6 us -> none  [the longest x1 31.8 us: regroup_weights(): lax.all_gather(stacked, 'sp', axis=0, tiled=False, axis_index_groups=inne...]
    ppermute x3 -> x0, waiting for transfers between devices: 25.5 us -> none  [regroup_weights(): piece = lax.ppermute(piece, 'sp', perm)]
    all_gather x1 -> x0, blocking collectives: 18.4 us -> none  [carried_in(): gathered = jax.tree.map(lambda a: lax.all_gather(a, axis), part)]
    dot_general x4 -> x0, other arithmetic: 14.2 us -> none  [block_update(): jnp.einsum('htk,hsk,htsk->hts', query_rows_block, gate_rows_block, decay_...]
    pallas_call x1, Pallas kernels: 84.9 us -> 98.1 us  [on_device(): pl.pallas_call(functools.partial(layer_kernel, sp_size, tp_size, up_piece...]
    ppermute x3 -> x0, starting transfers between devices: 6.14 us -> none  [regroup_weights(): piece = lax.ppermute(piece, 'sp', perm)]
    dot_general x13 -> x0, matrix products: 4.22 us -> none  [the longest x4 1.62 us: block_update(): jnp.einsum('tri,trw->tiw', gate_rows_block * jnp.exp(final_log_total - cu...]
    exp x5 -> x0, other arithmetic: 3.41 us -> none  [the longest x4 3.36 us: block_update(): decay_table = jnp.exp(jnp.where(causal[None, :, :, None], spread, -jnp.inf))]
  transfers between devices with their start and end apart: 6 -> 0, of which waited for: 4 -> 0; matrix products, arithmetic and copies ran while one was open for 3% -> 0% of each run, Pallas kernels for 0% -> 0%
where the time goes in v1:
time: 100 us; the launch traced here: 99.8 us
  Pallas kernels  98.1 us (98%)
  local copies, waits for them, and re-layouts  1.67 us (2%)
    pallas_call x1, Pallas kernels, on_device(): pl.pallas_call(functools.partial(layer_kernel, sp_size, tp_size, up_piece...  98.1 us

profile of v1, /device:TPU:0, one launch (start us, length us, event | category | flops | bytes accessed | tf_op | source)
XLA Modules:
  0.0 99.8 jit_solution(1648558488856493307)
XLA Ops:
  0.0 98.1 %shard_map.118 = bf16[64,2048]{1,0:T(8,128)(2,1)} custom-call(bf16[256,256]{1,0:T(8,128)(2,1)} %q_hbm.1, bf16[256,256]{1,0:T(8,128)(2,1)} %f_hbm.1, bf16[256,256]{1,0:T(8,128)(2,1)} %v_hbm.1, bf16[256,256]{1,0:T(8,128)(2,1)} %g_hbm.1, f32[1,256]{1,0:T(1,128)} %bitcast.4, f32[256,256]{1,0:T(8,128)} %ex_hbm.1, f32[1,128]{1,0:T(1,128)} %bitcast.5, ...), custom_call_target="tpu_custom_call" | custom-call | tf_op jit(solution)/shard_map/pallas_call | solution.py:569
  98.1 1.7 %copy.14 = bf16[64,2048]{1,0:T(8,128)(2,1)} copy(bf16[64,2048]{1,0:T(8,128)(2,1)} %shard_map.118) | data formatting | bytes 524288

commit v2 on v1

--- a/solution.py
+++ b/solution.py
@@ -28,8 +28,14 @@
     return [s * k for k in range(1, n) for s in (1, -1)]
 
 
+def pieces_of(rows):
+    return max(1, rows // 16)
+
+
 def by_distance(n):
-    return [sorted(range(n), key=lambda c: (abs(c - o), c)) for o in range(n)]
+    return [
+        sorted(range(n), key=lambda c: (abs(c - o), c if 2 * o < n else -c)) for o in range(n)
+    ]
 
 
 def dot_t(a, b):
@@ -50,10 +56,10 @@
     out_ref,
     qb, fb, vb, gb, exb, gapb, hgb, mgb, resb,
     cumb, gateb, recb, qcb, own, ownl, exc, excl, ss, sl, rs_, rl,
-    mixb, mx, wob, upb, dnb,
+    mixb, mx, wob, upb, dnb, s6, r6,
     stream, nb, pbuf, acc, s1, r1, s2, r2, acc2, s3, r3,
-    ldsem, sts, str_, lts, ltr, mxs, mxr, wos, wor, wfs, wfr, us, ur, fs, fr, dsn, dr,
-    zs, zr, hs, hr, ls, lr, ls2, lr2, q1s, q1r, q2s, q2r, q3s, q3r,
+    ldsem, sts, str_, lts, ltr, mxs, mxr, wos, wor, q6s, q6r, us, ur, fs, fr, dsn, dr,
+    zs, zr, hs, hr, ls, lr, q1s, q1r, q2s, q2r, q3s, q3r,
 ):
     outer, inner, hi = OUTER, sp_size // OUTER, tp_size // LO
     sp, tp = lax.axis_index("sp"), lax.axis_index("tp")
@@ -68,6 +74,8 @@
     down_rows = dn_hbm.shape[0]
     f32, b16 = jnp.float32, jnp.bfloat16
     steps = doubling(sp_size)
+    fine = pieces_of(rows)
+    part_rows = rows // fine
 
     def dev(ss_, tt):
         return (ss_, tt)
@@ -102,7 +110,7 @@
             [
                 (f_hbm, fb), (ex_hbm, exb), (gap_hbm, gapb), (v_hbm, vb), (q_hbm, qb), (g_hbm, gb),
                 (hg_hbm, hgb), (mg_hbm, mgb), (res_hbm, resb),
-                (wo_hbm, wob.at[tp]),
+                (wo_hbm, wob.at[l]),
                 (up_hbm.at[:, pl.ds(pl.multiple_of(o * width, width), width)], upb.at[sp]),
                 (dn_hbm, dnb.at[i]),
             ]
@@ -134,35 +142,32 @@
 
     def up_send(to, p):
         return rcopy(
-            up_cols(to, p), up_place(sp, p), us.at[to, p], ur.at[o, p], dev(to * inner + i, tp)
+            up_cols(to, p), up_place(sp, p), us, ur.at[o, p], dev(to * inner + i, tp)
         )
 
     def up_recv(source, p):
         place = up_place(source * inner + i, p)
-        return rcopy(place, place, us.at[source, p], ur.at[source, p], dev(source * inner + i, tp))
+        return rcopy(place, place, us, ur.at[source, p], dev(source * inner + i, tp))
 
     def fw_send(source, p, m, src):
         return rcopy(
-            src, up_place(source * inner + i, p), fs.at[source, p, m], fr.at[source, p, m],
+            src, up_place(source * inner + i, p), fs, fr,
             dev(o * inner + at_i(m), tp),
-        )
-
-    def fw_recv(source, p, m):
-        place = up_place(source * inner + from_i(m), p)
-        return rcopy(
-            place, place, fs.at[source, p, m], fr.at[source, p, m], dev(o * inner + from_i(m), tp)
         )
 
     def dn_send(p, m):
         part = pl.ds(p * dn_rows, dn_rows)
         return rcopy(
-            dn_hbm.at[part], dnb.at[i, part], dsn.at[p, m], dr.at[p, m],
+            dn_hbm.at[part], dnb.at[i, part], dsn, dr,
             dev(o * inner + at_i(m), tp),
         )
 
-    def dn_recv(p, m):
-        place = dnb.at[from_i(m), pl.ds(p * dn_rows, dn_rows)]
-        return rcopy(place, place, dsn.at[p, m], dr.at[p, m], dev(o * inner + from_i(m), tp))
+    def whole(ref, ssem, rsem):
+        return rcopy(ref, ref, ssem, rsem, dev(sp, at_t(1)))
+
+    fw_all = whole(upb.at[pl.ds(0, outer * (inner - 1))], fs, fr)
+    dn_all = whole(dnb.at[pl.ds(0, inner - 1)], dsn, dr)
+    up_all = whole(upb.at[pl.ds(0, outer - 1)], us, us)
 
     def inside(k):
         return (o + k >= 0) & (o + k < outer)
@@ -189,33 +194,20 @@
                 for m in range(1, inner):
                     fw_send(o + k, p, m, up_place((o + k) * inner + i, p)).start()
 
-    up_list = [(k, p) for k in hops(outer) for p in range(up_pieces)]
+    up_list = [(k, p) for k in hops(outer)[::-1] for p in range(up_pieces)]
     near = [(k, p) for k, p in up_list if abs(k) == 1]
-    groups = [[(k, p) for k, p in near if p == 0], [(k, p) for k, p in near if p > 0]]
     far = [(k, p) for k, p in up_list if abs(k) > 1]
-    groups += [[(k, p) for k, p in far if abs(k) == 2 and p == 0]]
-    rest = [it for it in far if it not in groups[2]]
-
-    def wo_send_l():
-        return rcopy(wo_hbm, wob.at[tp], wos.at[0], wor.at[0], dev(sp, h * LO + other))
-
-    def wo_send_h(m):
-        return rcopy(wo_hbm, wob.at[tp], wos.at[m], wor.at[m], dev(sp, at_h(m) * LO + l))
-
-    def wo_recv_h(m):
-        place = wob.at[from_h(m) * LO + l]
-        return rcopy(place, place, wos.at[m], wor.at[m], dev(sp, from_h(m) * LO + l))
-
-    def wo_fw(m):
-        place = wob.at[from_h(m) * LO + l]
-        return rcopy(place, place, wfs.at[m], wfr.at[m], dev(sp, h * LO + other))
-
-    wo_send_l().start()
-    for m in range(1, hi):
-        wo_send_h(m).start()
-    own_issue(0)
-    up_issue(groups[0])
-
+    falling = [(k, p) for k, p in up_list if k < 0]
+    rising = [(k, p) for k, p in up_list[::-1] if k > 0]
+
+    def piece(q):
+        return pl.ds(q * part_rows, part_rows)
+
+    def wo_copy():
+        return rcopy(wo_hbm, wob.at[l], wos, wor, dev(sp, h * LO + other))
+
+    wo_copy().start()
+    up_issue(falling)
     for c in loads[:4]:
         c.wait()
     gate = gapb[...] / (1.0 + jnp.exp(fb[...].astype(f32)))
@@ -271,8 +263,7 @@
             sl[n, k : k + 1, :] = ownl[k : k + 1, :] + excl[k : k + 1, :]
 
     step_send(0)
-    up_issue(groups[1])
-    for p in range(1, up_pieces):
+    for p in range(up_pieces):
         own_issue(p)
     for p in range(down_pieces):
         dn_issue(p)
@@ -308,13 +299,10 @@
         if n + 1 < len(steps):
             step_pack(n + 1)
             step_send(n + 1)
-            if n == 0:
-                up_issue(groups[2])
             if n + 2 == len(steps):
-                up_issue(rest)
+                up_issue(rising)
     if len(steps) < 2:
-        up_issue(groups[2])
-        up_issue(rest)
+        up_issue(rising)
 
     loads[5].wait()
     loads[6].wait()
@@ -326,40 +314,38 @@
         mixed = (normal * hgb[...] * (logits / (1.0 + jnp.exp(-logits)))).astype(b16)
         mixb[:, :, at] = mixed.reshape(tp_size, rows, HEAD_V)
 
-    def mx_send(m):
-        return rcopy(mixb.at[at_t(m)], mx.at[tp], mxs.at[m], mxr.at[m], dev(sp, at_t(m)))
-
-    def mx_recv(m):
-        place = mx.at[from_t(m)]
-        return rcopy(place, place, mxs.at[m], mxr.at[m], dev(sp, from_t(m)))
-
-    for m in range(1, tp_size):
-        mx_send(m).start()
-    mx[tp] = mixb[tp]
-    fw_issue(near)
-
-    for m in range(1, hi):
-        wo_recv_h(m).wait_recv()
-        wo_fw(m).start()
-    for m in range(1, tp_size):
-        mx_recv(m).wait_recv()
+    def mx_copy(hh):
+        return rcopy(
+            mixb.at[hh * LO + other], mx.at[l, hh], mxs, mxr, dev(sp, h * LO + other)
+        )
+
+    def p6_copy(m, q):
+        return rcopy(
+            s6.at[m, piece(q)], r6.at[m, piece(q)], q6s, q6r.at[m - 1, q],
+            dev(sp, at_h(m) * LO + l),
+        )
+
+    for hh in range(hi):
+        mx_copy(hh).start()
+    for hh in range(hi):
+        mx[l, hh] = mixb[hh * LO + l]
     for c in loads[7:10]:
         c.wait()
-    wo_send_l().wait_recv()
-    total = resb[...].astype(f32)
-    for ll in range(LO):
-        t = h * LO + ll
-        total = total + dot(mx[t], wob[t])
+    wo_copy().wait_recv()
+    mx_all = whole(mx.at[0], mxs, mxr)
+    mx_all.wait_recv()
+
+    def projected(hh):
+        got = dot(mx[0, hh], wob[0])
+        for ll in range(1, LO):
+            got = got + dot(mx[ll, hh], wob[ll])
+        return got
+
     for m in range(1, hi):
-        t = from_h(m) * LO + l
-        total = total + dot(mx[t], wob[t])
-    for m in range(1, hi):
-        wo_fw(m).wait_recv()
-        t = from_h(m) * LO + other
-        total = total + dot(mx[t], wob[t])
-    stream[...] = total
-    scale = lax.rsqrt(jnp.mean(total * total, axis=-1, keepdims=True) + norm_eps)
-    nb[o, tp] = (total * scale * mgb[...]).astype(b16)
+        s6[m] = projected(at_h(m)).astype(b16)
+        for q in range(fine):
+            p6_copy(m, q).start()
+    stream[...] = resb[...].astype(f32) + projected(h)
 
     table = by_distance(outer)
 
@@ -370,79 +356,105 @@
                 c = jnp.where((o == oo) & (p == pp), table[oo][pp], c)
         return c
 
-    def z_copy(c, to):
-        ref = nb.at[c, tp]
-        return rcopy(ref, ref, zs.at[c, to], zr.at[c], dev(to * inner + i, tp))
-
-    def h_copy(c, m):
-        ref = nb.at[c, tp]
-        return rcopy(ref, ref, hs.at[c, m], hr.at[c, m], dev(sp, at_h(m) * LO + l))
-
-    def l_copy(c):
-        ref = nb.at[c, tp]
-        return rcopy(ref, ref, ls.at[c], lr.at[c], dev(sp, h * LO + other))
-
-    def l2_copy(c, m):
-        ref = nb.at[c, from_h(m) * LO + l]
-        return rcopy(ref, ref, ls2.at[c, m], lr2.at[c, m], dev(sp, h * LO + other))
-
-    def pass_up(c):
+    def z_copy(c, q, to):
+        ref = nb.at[c, tp, piece(q)]
+        return rcopy(ref, ref, zs.at[c, jnp.where(to > o, 1, 0)], zr.at[c, q], dev(to * inner + i, tp))
+
+    def h_copy(c, q, m):
+        ref = nb.at[c, tp, piece(q)]
+        return rcopy(ref, ref, hs, hr.at[c, m - 1, q], dev(sp, at_h(m) * LO + l))
+
+    def l_copy(c, q):
+        ref = nb.at[c, tp, piece(q)]
+        return rcopy(ref, ref, ls, lr.at[c], dev(sp, h * LO + other))
+
+    def l2_copy(c, q, m):
+        ref = nb.at[c, from_h(m) * LO + l, piece(q)]
+        return rcopy(ref, ref, ls, lr.at[c], dev(sp, h * LO + other))
+
+    def pass_on(c, q):
         @pl.when((c <= o) & (o + 1 < outer))
         def _():
-            z_copy(c, o + 1).start()
+            z_copy(c, q, o + 1).start()
 
         @pl.when((c >= o) & (o > 0))
         def _():
-            z_copy(c, o - 1).start()
-
-    def spread(c):
+            z_copy(c, q, o - 1).start()
+
+    def spread(c, q):
         for m in range(1, hi):
-            h_copy(c, m).start()
-        l_copy(c).start()
-
-    def gather(c):
+            h_copy(c, q, m).start()
+        l_copy(c, q).start()
+
+    def gather(c, q):
         for m in range(1, hi):
-            h_copy(c, m).wait_recv()
-            l2_copy(c, m).start()
-
-    pass_up(o)
-    spread(o)
-    fw_issue(groups[2] + rest)
-
-    def ag_body(p, carry):
+            h_copy(c, q, m).wait_recv()
+            l2_copy(c, q, m).start()
+
+    for q in range(fine):
+        r = slice(q * part_rows, (q + 1) * part_rows)
+        total = stream[r]
+        for m in range(1, hi):
+            p6_copy(m, q).wait_recv()
+            total = total + r6[m, r].astype(f32)
+        stream[r] = total
+        scale = lax.rsqrt(jnp.mean(total * total, axis=-1, keepdims=True) + norm_eps)
+        nb[o, tp, r] = (total * scale * mgb[...]).astype(b16)
+        pass_on(o, q)
+        spread(o, q)
+
+    for p in range(1, outer):
         c = chunk_at(p)
-        z_copy(c, o).wait_recv()
-        pass_up(c)
-        spread(c)
-        gather(chunk_at(p - 1))
-        return carry
-
-    lax.fori_loop(1, outer, ag_body, 0)
-    gather(chunk_at(outer - 1))
+        for q in range(fine):
+            z_copy(c, q, o).wait_recv()
+            pass_on(c, q)
+            spread(c, q)
+            gather(chunk_at(p - 1), q)
+            if p == 1:
+                fw_issue(([near] + [far[n :: fine - 1] for n in range(fine - 1)])[q] if fine > 1 else near + far)
+    for q in range(fine):
+        gather(chunk_at(outer - 1), q)
 
     for c in loads[10:]:
         c.wait()
-    for k in [0] + hops(outer):
-        @pl.when(inside(k))
-        def _():
-            for p in range(up_pieces):
-                for m in range(1, inner):
-                    fw_recv(o + k, p, m).wait_recv()
-    for p in range(down_pieces):
-        for m in range(1, inner):
-            dn_recv(p, m).wait_recv()
+    fw_all.wait_recv()
+    dn_all.wait_recv()
 
     def s1_copy(k):
-        return rcopy(s1.at[k], r1.at[k], q1s.at[k], q1r.at[k], dev(sp, h * LO + other))
-
-    def s2_copy(k, m):
-        return rcopy(s2.at[k, m], r2.at[k, m], q2s.at[k, m], q2r.at[k, m], dev(sp, at_h(m) * LO + l))
-
-    def s3_copy(c):
-        return rcopy(s3.at[c], r3.at[o], q3s.at[c], q3r.at[o], dev(c * inner + i, tp))
-
-    def s3_recv(c):
-        return rcopy(r3.at[c], r3.at[c], q3s.at[c], q3r.at[c], dev(c * inner + i, tp))
+        return rcopy(s1.at[k], r1.at[k], q1s, q1r.at[k], dev(sp, h * LO + other))
+
+    def s2_copy(k, m, q):
+        return rcopy(
+            s2.at[k, m, piece(q)], r2.at[k, m, piece(q)], q2s, q2r.at[k, m - 1, q],
+            dev(sp, at_h(m) * LO + l),
+        )
+
+    def before(c):
+        return jnp.where(c > o, o > 0, o + 1 < outer)
+
+    def s3_copy(c, q):
+        to = jnp.where(c > o, o + 1, o - 1)
+        slot = jnp.where((c < o) & (c == to), outer, c)
+        return rcopy(
+            s3.at[c, piece(q)], r3.at[slot, piece(q)], q3s, q3r.at[slot, q],
+            dev(to * inner + i, tp),
+        )
+
+    def s3_recv(slot, q):
+        place = r3.at[slot, piece(q)]
+        return rcopy(place, place, q3s, q3r.at[slot, q], dev(sp, at_t(1)))
+
+    def relay(k, q):
+        c = turn(k)
+        r = slice(q * part_rows, (q + 1) * part_rows)
+
+        @pl.when(before(c))
+        def _():
+            s3_recv(c, q).wait_recv()
+            acc2[k, r] = acc2[k, r] + r3[c, r].astype(f32)
+
+        s3[c, r] = acc2[k, r].astype(b16)
+        s3_copy(c, q).start()
 
     def turn(j):
         return chunk_at(outer - 1 - j)
@@ -451,9 +463,7 @@
         @pl.when(j < outer)
         def _():
             c = turn(j)
-            l_copy(c).wait_recv()
-            for m in range(1, hi):
-                l2_copy(c, m).wait_recv()
+            whole(nb.at[c, pl.ds(0, hi)], ls, lr.at[c]).wait_recv()
             x = nb[c].reshape(tp_size * rows, depth)
             lifted = dot(x, upb[...].reshape(depth, width))
             hidden = jnp.square(jnp.maximum(lifted, 0.0)).astype(b16)
@@ -465,85 +475,83 @@
             for hh in range(hi):
                 acc[j, hh] = pbuf[hh * LO + l]
 
-        @pl.when((j >= 1) & (j < outer + 1))
+        @pl.when(j >= 1)
         def _():
             k = j - 1
             s1_copy(k).wait_recv()
             for m in range(1, hi):
                 to = at_h(m)
-                s2[k, m] = (acc[k, to] + r1[k, to].astype(f32)).astype(b16)
-                s2_copy(k, m).start()
+                for q in range(fine):
+                    r = slice(q * part_rows, (q + 1) * part_rows)
+                    s2[k, m, r] = (acc[k, to, r] + r1[k, to, r].astype(f32)).astype(b16)
+                    s2_copy(k, m, q).start()
             acc2[k] = acc[k, h] + r1[k, h].astype(f32)
 
-        @pl.when(j >= 2)
-        def _():
-            k = j - 2
-            v = acc2[k]
+        return carry
+
+    lax.fori_loop(0, outer + 1, body, 0)
+
+    for k in range(outer):
+        for q in range(fine):
+            r = slice(q * part_rows, (q + 1) * part_rows)
+            v = acc2[k, r]
             for m in range(1, hi):
-                s2_copy(k, m).wait_recv()
-                v = v + r2[k, m].astype(f32)
-
-            @pl.when(k < outer - 1)
-            def _():
-                c = turn(k)
-                s3[c] = v.astype(b16)
-                s3_copy(c).start()
-
-            @pl.when(k == outer - 1)
-            def _():
-                stream[...] = stream[...] + v
-
-        return carry
-
-    lax.fori_loop(0, outer + 2, body, 0)
-    final = stream[...]
-    for k in range(1, outer):
-        c = chunk_at(k)
-        s3_recv(c).wait_recv()
-        final = final + r3[c].astype(f32)
-    out_ref[...] = final.astype(b16)
-
-    wo_send_l().wait_send()
-    for m in range(1, hi):
-        wo_send_h(m).wait_send()
-        wo_fw(m).wait_send()
-    for m in range(1, tp_size):
-        mx_send(m).wait_send()
+                s2_copy(k, m, q).wait_recv()
+                v = v + r2[k, m, r].astype(f32)
+            acc2[k, r] = v
+            if 0 < k < outer - 1:
+                @pl.when(before(turn(k - 1)))
+                def _():
+                    relay(k - 1, q)
+            if k == outer - 2:
+                relay(k, q)
+            elif k < outer - 2:
+                @pl.when(jnp.logical_not(before(turn(k))))
+                def _():
+                    relay(k, q)
+
+    for q in range(fine):
+        r = slice(q * part_rows, (q + 1) * part_rows)
+        final = stream[r] + acc2[outer - 1, r]
+        stream[r] = final
+
+        @pl.when(o > 0)
+        def _():
+            s3_recv(o, q).wait_recv()
+            stream[r] = stream[r] + r3[o, r].astype(f32)
+
+        @pl.when(o + 1 < outer)
+        def _():
+            s3_recv(outer, q).wait_recv()
+            stream[r] = stream[r] + r3[outer, r].astype(f32)
+
+        out_ref[r] = stream[r].astype(b16)
+
+    wo_copy().wait_send()
+    mx_all.wait_send()
+    whole(s6.at[pl.ds(0, hi - 1)], q6s, q6s).wait_send()
     for n in range(len(steps)):
         @pl.when(sp + steps[n] < sp_size)
         def _():
             lt_send(n).wait_send()
             st_send(n).wait_send()
-    for k, p in up_list:
-        @pl.when(inside(k))
-        def _():
-            up_send(o + k, p).wait_send()
-            for m in range(1, inner):
-                fw_send(o + k, p, m, up_place((o + k) * inner + i, p)).wait_send()
-    for m in range(1, inner):
-        for p in range(up_pieces):
-            fw_send(o, p, m, up_cols(o, p)).wait_send()
-        for p in range(down_pieces):
-            dn_send(p, m).wait_send()
+    up_all.wait_send()
+    fw_all.wait_send()
+    dn_all.wait_send()
     for c in range(outer):
         @pl.when((c <= o) & (o + 1 < outer))
         def _():
-            z_copy(c, o + 1).wait_send()
+            whole(nb.at[c, tp], zs.at[c, 1], zs.at[c, 1]).wait_send()
 
         @pl.when((c >= o) & (o > 0))
         def _():
-            z_copy(c, o - 1).wait_send()
-
-        @pl.when(c != o)
-        def _():
-            s3_copy(c).wait_send()
-
-        l_copy(c).wait_send()
-        s1_copy(c).wait_send()
-        for m in range(1, hi):
-            h_copy(c, m).wait_send()
-            l2_copy(c, m).wait_send()
-            s2_copy(c, m).wait_send()
+            whole(nb.at[c, tp], zs.at[c, 0], zs.at[c, 0]).wait_send()
+
+    whole(s1.at[:, pl.ds(0, hi - 1)], hs, hs).wait_send()
+    whole(s1, ls, ls).wait_send()
+    whole(s1, q1s, q1s).wait_send()
+    whole(s2.at[:, pl.ds(0, hi - 1)], q2s, q2s).wait_send()
+    whole(s3.at[pl.ds(0, outer - 1)], q3s, q3s).wait_send()
 
 
 def on_device(
@@ -564,7 +572,7 @@
     f32, b16 = jnp.float32, jnp.bfloat16
     dma = pltpu.SemaphoreType.DMA
     vm = pltpu.VMEM
-    O = OUTER
+    O, F = OUTER, pieces_of(rows)
     lrows = 8 * ((heads + 7) // 8)
     return pl.pallas_call(
         functools.partial(layer_kernel, sp_size, tp_size, up_pieces, down_pieces),
@@ -583,10 +591,11 @@
             vm((heads, HEAD_V, HEAD_K), f32), vm((lrows, HEAD_K), f32),
             vm((steps, heads, HEAD_V, HEAD_K), b16), vm((steps, lrows, HEAD_K), f32),
             vm((steps, heads, HEAD_V, HEAD_K), b16), vm((steps, lrows, HEAD_K), f32),
-            vm((tp_size, rows, local_width), b16), vm((tp_size, rows, local_width), b16),
-            vm((tp_size, local_width, depth), b16),
+            vm((tp_size, rows, local_width), b16), vm((LO, hi, rows, local_width), b16),
+            vm((LO, local_width, depth), b16),
             vm((sp_size, depth_part, width), b16),
             vm((inner, down_rows, depth), b16),
+            vm((hi, rows, depth), b16), vm((hi, rows, depth), b16),
             vm((rows, depth), f32),
             vm((O, tp_size, rows, depth), b16),
             vm((tp_size, rows, depth), f32),
@@ -594,19 +603,18 @@
             vm((O, hi, rows, depth), b16), vm((O, hi, rows, depth), b16),
             vm((O, hi, rows, depth), b16), vm((O, hi, rows, depth), b16),
             vm((O, rows, depth), f32),
-            vm((O, rows, depth), b16), vm((O, rows, depth), b16),
+            vm((O, rows, depth), b16), vm((O + 1, rows, depth), b16),
             dma((12,)),
             dma((steps,)), dma((steps,)), dma((steps,)), dma((steps,)),
-            dma((tp_size,)), dma((tp_size,)),
-            dma((hi,)), dma((hi,)), dma((hi,)), dma((hi,)),
-            dma((O, up_pieces)), dma((O, up_pieces)),
-            dma((O, up_pieces, inner)), dma((O, up_pieces, inner)),
-            dma((down_pieces, inner)), dma((down_pieces, inner)),
-            dma((O, O)), dma((O,)),
-            dma((O, hi)), dma((O, hi)),
-            dma((O,)), dma((O,)), dma((O, hi)), dma((O, hi)),
-            dma((O,)), dma((O,)), dma((O, hi)), dma((O, hi)),
-            dma((O,)), dma((O,)),
+            dma, dma, dma, dma,
+            dma, dma((hi - 1, F)),
+            dma, dma((O, up_pieces)),
+            dma, dma, dma, dma,
+            dma((O, 2)), dma((O, F)),
+            dma, dma((O, hi - 1, F)),
+            dma, dma((O,)),
+            dma, dma((O,)), dma, dma((O, hi - 1, F)),
+            dma, dma((O + 1, F)),
         ],
         compiler_params=pltpu.CompilerParams(
             collective_id=0, has_side_effects=True, vmem_limit_bytes=60 * 1024 * 1024

time: 100 us -> 86 us (0.86)
  Pallas kernels: 98.1 us -> 83.3 us
    pallas_call x1, Pallas kernels: 98.1 us -> 83.3 us  [on_device(): pl.pallas_call(functools.partial(layer_kernel, sp_size, tp_size, up_piece...]
where the time goes in v2:
time: 86 us; the launch traced here: 85 us
  Pallas kernels  83.3 us (97%)
  local copies, waits for them, and re-layouts  1.67 us (2%)
    pallas_call x1, Pallas kernels, on_device(): pl.pallas_call(functools.partial(layer_kernel, sp_size, tp_size, up_piece...  83.3 us

profile of v2, /device:TPU:0, one launch (start us, length us, event | category | flops | bytes accessed | tf_op | source)
XLA Modules:
  0.0 85.0 jit_solution(18391787053882905320)
XLA Ops:
  0.0 83.3 %shard_map.118 = bf16[64,2048]{1,0:T(8,128)(2,1)} custom-call(bf16[256,256]{1,0:T(8,128)(2,1)} %q_hbm.1, bf16[256,256]{1,0:T(8,128)(2,1)} %f_hbm.1, bf16[256,256]{1,0:T(8,128)(2,1)} %v_hbm.1, bf16[256,256]{1,0:T(8,128)(2,1)} %g_hbm.1, f32[1,256]{1,0:T(1,128)} %bitcast.4, f32[256,256]{1,0:T(8,128)} %ex_hbm.1, f32[1,128]{1,0:T(1,128)} %bitcast.5, ...), custom_call_target="tpu_custom_call" | custom-call | tf_op jit(solution)/shard_map/pallas_call | solution.py:577
  83.3 1.7 %copy.14 = bf16[64,2048]{1,0:T(8,128)(2,1)} copy(bf16[64,2048]{1,0:T(8,128)(2,1)} %shard_map.118) | data formatting | bytes 524288

commit v3 on v2

--- a/solution.py
+++ b/solution.py
@@ -32,6 +32,10 @@
     return max(1, rows // 16)
 
 
+def halves_of(rows):
+    return max(1, rows // 32)
+
+
 def by_distance(n):
     return [
         sorted(range(n), key=lambda c: (abs(c - o), c if 2 * o < n else -c)) for o in range(n)
@@ -57,7 +61,7 @@
     qb, fb, vb, gb, exb, gapb, hgb, mgb, resb,
     cumb, gateb, recb, qcb, own, ownl, exc, excl, ss, sl, rs_, rl,
     mixb, mx, wob, upb, dnb, s6, r6,
-    stream, nb, pbuf, acc, s1, r1, s2, r2, acc2, s3, r3,
+    stream, nb, hid, pbuf, acc, s1, r1, s2, r2, acc2, s3, r3,
     ldsem, sts, str_, lts, ltr, mxs, mxr, wos, wor, q6s, q6r, us, ur, fs, fr, dsn, dr,
     zs, zr, hs, hr, ls, lr, q1s, q1r, q2s, q2r, q3s, q3r,
 ):
@@ -76,6 +80,9 @@
     steps = doubling(sp_size)
     fine = pieces_of(rows)
     part_rows = rows // fine
+    coarse = halves_of(rows)
+    sum_rows = rows // coarse
+    half = depth // 2
 
     def dev(ss_, tt):
         return (ss_, tt)
@@ -155,18 +162,21 @@
             dev(o * inner + at_i(m), tp),
         )
 
-    def dn_send(p, m):
-        part = pl.ds(p * dn_rows, dn_rows)
+    def dn_send(n, p, m):
+        part, at = pl.ds(p * dn_rows, dn_rows), pl.ds(n * half, half)
         return rcopy(
-            dn_hbm.at[part], dnb.at[i, part], dsn, dr,
-            dev(o * inner + at_i(m), tp),
+            dn_hbm.at[part, at], dnb.at[i, part, at], dsn, dr.at[n], dev(o * inner + at_i(m), tp)
         )
 
     def whole(ref, ssem, rsem):
         return rcopy(ref, ref, ssem, rsem, dev(sp, at_t(1)))
 
     fw_all = whole(upb.at[pl.ds(0, outer * (inner - 1))], fs, fr)
-    dn_all = whole(dnb.at[pl.ds(0, inner - 1)], dsn, dr)
+    dn_all = whole(dnb.at[pl.ds(0, inner - 1)], dsn, dsn)
+
+    def dn_half(n):
+        return whole(dnb.at[pl.ds(0, inner - 1), :, pl.ds(n * half, half)], dsn, dr.at[n])
+
     up_all = whole(upb.at[pl.ds(0, outer - 1)], us, us)
 
     def inside(k):
@@ -182,9 +192,12 @@
         for m in range(1, inner):
             fw_send(o, p, m, up_cols(o, p)).start()
 
-    def dn_issue(p):
-        for m in range(1, inner):
-            dn_send(p, m).start()
+    def dn_issue(items):
+        for n, p in items:
+            for m in range(1, inner):
+                dn_send(n, p, m).start()
+
+    dn_list = [(n, p) for n in range(2) for p in range(down_pieces)]
 
     def fw_issue(items):
         for k, p in items:
@@ -198,7 +211,8 @@
     near = [(k, p) for k, p in up_list if abs(k) == 1]
     far = [(k, p) for k, p in up_list if abs(k) > 1]
     falling = [(k, p) for k, p in up_list if k < 0]
-    rising = [(k, p) for k, p in up_list[::-1] if k > 0]
+    rising = [(k, p) for k, p in near if k > 0]
+    rising_far = [(k, p) for k, p in far if k > 0]
 
     def piece(q):
         return pl.ds(q * part_rows, part_rows)
@@ -263,10 +277,10 @@
             sl[n, k : k + 1, :] = ownl[k : k + 1, :] + excl[k : k + 1, :]
 
     step_send(0)
+    up_issue(rising[:1])
     for p in range(up_pieces):
         own_issue(p)
-    for p in range(down_pieces):
-        dn_issue(p)
+    dn_issue(dn_list[:-1])
 
     loads[4].wait()
     scaled = qb[...].astype(f32) * HEAD_K ** (-0.5)
@@ -299,10 +313,18 @@
         if n + 1 < len(steps):
             step_pack(n + 1)
             step_send(n + 1)
+            if n == 0:
+                up_issue(rising[1:])
             if n + 2 == len(steps):
-                up_issue(rising)
+                @pl.when(o > 0)
+                def _():
+                    up_issue(rising_far)
     if len(steps) < 2:
-        up_issue(rising)
+        up_issue(rising[1:])
+
+        @pl.when(o > 0)
+        def _():
+            up_issue(rising_far)
 
     loads[5].wait()
     loads[6].wait()
@@ -403,6 +425,10 @@
         pass_on(o, q)
         spread(o, q)
 
+    @pl.when(o == 0)
+    def _():
+        up_issue(rising_far)
+
     for p in range(1, outer):
         c = chunk_at(p)
         for q in range(fine):
@@ -410,122 +436,160 @@
             pass_on(c, q)
             spread(c, q)
             gather(chunk_at(p - 1), q)
-            if p == 1:
-                fw_issue(([near] + [far[n :: fine - 1] for n in range(fine - 1)])[q] if fine > 1 else near + far)
-    for q in range(fine):
-        gather(chunk_at(outer - 1), q)
+            if p == 1 and q == 0:
+                fw_issue(near)
+            if p == 1 and q == fine // 2:
+                fw_issue([it for it in far if it[0] > 0])
+        if p == 1:
+            fw_issue([it for it in far if it[0] < 0])
+            dn_issue(dn_list[-1:])
+    def gather_last():
+        for q in range(fine):
+            gather(chunk_at(outer - 1), q)
 
     for c in loads[10:]:
         c.wait()
     fw_all.wait_recv()
-    dn_all.wait_recv()
+    dn_half(0).wait_recv()
 
     def s1_copy(k):
         return rcopy(s1.at[k], r1.at[k], q1s, q1r.at[k], dev(sp, h * LO + other))
 
+    def rows_of(q):
+        return slice(q * sum_rows, (q + 1) * sum_rows)
+
     def s2_copy(k, m, q):
+        r = pl.ds(q * sum_rows, sum_rows)
         return rcopy(
-            s2.at[k, m, piece(q)], r2.at[k, m, piece(q)], q2s, q2r.at[k, m - 1, q],
+            s2.at[k, m - 1, r], r2.at[k, m - 1, r], q2s, q2r.at[k, m - 1, q],
             dev(sp, at_h(m) * LO + l),
         )
 
     def before(c):
         return jnp.where(c > o, o > 0, o + 1 < outer)
 
-    def s3_copy(c, q):
+    def s3_copy(n, c, q):
         to = jnp.where(c > o, o + 1, o - 1)
         slot = jnp.where((c < o) & (c == to), outer, c)
+        r = pl.ds(q * sum_rows, sum_rows)
         return rcopy(
-            s3.at[c, piece(q)], r3.at[slot, piece(q)], q3s, q3r.at[slot, q],
-            dev(to * inner + i, tp),
-        )
-
-    def s3_recv(slot, q):
-        place = r3.at[slot, piece(q)]
-        return rcopy(place, place, q3s, q3r.at[slot, q], dev(sp, at_t(1)))
+            s3.at[n, c, r], r3.at[n, slot, r], q3s, q3r.at[n, slot, q], dev(to * inner + i, tp)
+        )
+
+    def s3_recv(n, slot, q):
+        place = r3.at[n, slot, pl.ds(q * sum_rows, sum_rows)]
+        return rcopy(place, place, q3s, q3r.at[n, slot, q], dev(sp, at_t(1)))
 
     def relay(k, q):
-        c = turn(k)
-        r = slice(q * part_rows, (q + 1) * part_rows)
+        n, c, r = half_of(k), turn(k), rows_of(q)
 
         @pl.when(before(c))
         def _():
-            s3_recv(c, q).wait_recv()
-            acc2[k, r] = acc2[k, r] + r3[c, r].astype(f32)
-
-        s3[c, r] = acc2[k, r].astype(b16)
-        s3_copy(c, q).start()
+            s3_recv(n, c, q).wait_recv()
+            acc2[k, r] = acc2[k, r] + r3[n, c, r].astype(f32)
+
+        s3[n, c, r] = acc2[k, r].astype(b16)
+        s3_copy(n, c, q).start()
+
+    slots, lag = 2 * outer, 3
 
     def turn(j):
-        return chunk_at(outer - 1 - j)
+        p = jnp.where((j == 0) | (j == slots - 3), 1, outer - 1 - (j - 1) // 2)
+        return chunk_at(jnp.where(j >= slots - 2, 0, p))
+
+    def half_of(j):
+        return jnp.where(j >= slots - 3, jnp.where(j == slots - 2, 0, 1), jnp.where(j == 0, 0, lax.rem(j + 1, 2)))
+
+    def send_sums(k):
+        s1_copy(k).wait_recv()
+        for m in range(1, hi):
+            to = at_h(m)
+            for q in range(coarse):
+                r = rows_of(q)
+                s2[k, m - 1, r] = (acc[k, to, r] + r1[k, to, r].astype(f32)).astype(b16)
+                s2_copy(k, m, q).start()
+        acc2[k] = acc[k, h] + r1[k, h].astype(f32)
+
+    def collect(k):
+        for q in range(coarse):
+            r = rows_of(q)
+            v = acc2[k, r]
+            for m in range(1, hi):
+                s2_copy(k, m, q).wait_recv()
+                v = v + r2[k, m - 1, r].astype(f32)
+            acc2[k, r] = v
+
+            @pl.when((k < slots - 2) & jnp.logical_not(before(turn(k))))
+            def _():
+                relay(k, q)
+
+            @pl.when((k == slots - 3) & before(turn(0)))
+            def _():
+                relay(0, q)
+
+            @pl.when((k >= 2) & (k < slots - 1) & before(turn(k - 1)))
+            def _():
+                relay(k - 1, q)
 
     def body(j, carry):
-        @pl.when(j < outer)
+        @pl.when(j == 1)
+        def _():
+            send_sums(0)
+            gather_last()
+
+        @pl.when(j < slots)
         def _():
             c = turn(j)
-            whole(nb.at[c, pl.ds(0, hi)], ls, lr.at[c]).wait_recv()
-            x = nb[c].reshape(tp_size * rows, depth)
-            lifted = dot(x, upb[...].reshape(depth, width))
-            hidden = jnp.square(jnp.maximum(lifted, 0.0)).astype(b16)
-            part = dot(hidden, dnb[...].reshape(width, depth))
-            pbuf[...] = part.reshape(tp_size, rows, depth)
+
+            @pl.when((j == 0) | (j == slots - 2) | ((j < slots - 3) & (lax.rem(j, 2) == 1)))
+            def _():
+                whole(nb.at[c, pl.ds(0, hi)], ls, lr.at[c]).wait_recv()
+                x = nb[c].reshape(tp_size * rows, depth)
+                lifted = dot(x, upb[...].reshape(depth, width))
+                hid[c] = jnp.square(jnp.maximum(lifted, 0.0)).astype(b16)
+
+            @pl.when(j == 2)
+            def _():
+                dn_half(1).wait_recv()
+
+            at = pl.ds(pl.multiple_of(half_of(j) * half, half), half)
+            part = dot(hid[c], dnb[:, :, at].reshape(width, half))
+            pbuf[...] = part.reshape(tp_size, rows, half)
             for hh in range(hi):
                 s1[j, hh] = pbuf[hh * LO + other].astype(b16)
             s1_copy(j).start()
             for hh in range(hi):
                 acc[j, hh] = pbuf[hh * LO + l]
 
-        @pl.when(j >= 1)
-        def _():
-            k = j - 1
-            s1_copy(k).wait_recv()
-            for m in range(1, hi):
-                to = at_h(m)
-                for q in range(fine):
-                    r = slice(q * part_rows, (q + 1) * part_rows)
-                    s2[k, m, r] = (acc[k, to, r] + r1[k, to, r].astype(f32)).astype(b16)
-                    s2_copy(k, m, q).start()
-            acc2[k] = acc[k, h] + r1[k, h].astype(f32)
+        @pl.when((j >= 2) & (j < slots + 1))
+        def _():
+            send_sums(j - 1)
+
+        @pl.when(j >= lag)
+        def _():
+            collect(j - lag)
 
         return carry
 
-    lax.fori_loop(0, outer + 1, body, 0)
-
-    for k in range(outer):
-        for q in range(fine):
-            r = slice(q * part_rows, (q + 1) * part_rows)
-            v = acc2[k, r]
-            for m in range(1, hi):
-                s2_copy(k, m, q).wait_recv()
-                v = v + r2[k, m, r].astype(f32)
-            acc2[k, r] = v
-            if 0 < k < outer - 1:
-                @pl.when(before(turn(k - 1)))
-                def _():
-                    relay(k - 1, q)
-            if k == outer - 2:
-                relay(k, q)
-            elif k < outer - 2:
-                @pl.when(jnp.logical_not(before(turn(k))))
-                def _():
-                    relay(k, q)
-
-    for q in range(fine):
-        r = slice(q * part_rows, (q + 1) * part_rows)
-        final = stream[r] + acc2[outer - 1, r]
-        stream[r] = final
-
-        @pl.when(o > 0)
-        def _():
-            s3_recv(o, q).wait_recv()
-            stream[r] = stream[r] + r3[o, r].astype(f32)
-
-        @pl.when(o + 1 < outer)
-        def _():
-            s3_recv(outer, q).wait_recv()
-            stream[r] = stream[r] + r3[outer, r].astype(f32)
-
-        out_ref[r] = stream[r].astype(b16)
+    lax.fori_loop(0, slots + lag, body, 0)
+
+    for n in range(2):
+        at = slice(n * half, (n + 1) * half)
+        mine = slots - 2 + n
+        for q in range(coarse):
+            r = rows_of(q)
+
+            @pl.when(o > 0)
+            def _():
+                s3_recv(n, o, q).wait_recv()
+                acc2[mine, r] = acc2[mine, r] + r3[n, o, r].astype(f32)
+
+            @pl.when(o + 1 < outer)
+            def _():
+                s3_recv(n, outer, q).wait_recv()
+                acc2[mine, r] = acc2[mine, r] + r3[n, outer, r].astype(f32)
+
+            out_ref[r, at] = (stream[r, at] + acc2[mine, r]).astype(b16)
 
     wo_copy().wait_send()
     mx_all.wait_send()
@@ -550,8 +614,8 @@
     whole(s1.at[:, pl.ds(0, hi - 1)], hs, hs).wait_send()
     whole(s1, ls, ls).wait_send()
     whole(s1, q1s, q1s).wait_send()
-    whole(s2.at[:, pl.ds(0, hi - 1)], q2s, q2s).wait_send()
-    whole(s3.at[pl.ds(0, outer - 1)], q3s, q3s).wait_send()
+    whole(s2, q2s, q2s).wait_send()
+    whole(s3.at[:, pl.ds(0, outer - 1)], q3s, q3s).wait_send()
 
 
 def on_device(
@@ -567,12 +631,12 @@
     inner, hi = sp_size // OUTER, tp_size // LO
     width = cols // OUTER
     up_pieces = max(1, min(2, depth_part // 128))
-    down_pieces = max(1, min(4, down_rows // 64))
+    down_pieces = max(1, min(2, down_rows // 64))
     steps = len(doubling(sp_size))
     f32, b16 = jnp.float32, jnp.bfloat16
     dma = pltpu.SemaphoreType.DMA
     vm = pltpu.VMEM
-    O, F = OUTER, pieces_of(rows)
+    O, F, C, half = OUTER, pieces_of(rows), halves_of(rows), depth // 2
     lrows = 8 * ((heads + 7) // 8)
     return pl.pallas_call(
         functools.partial(layer_kernel, sp_size, tp_size, up_pieces, down_pieces),
@@ -598,23 +662,24 @@
             vm((hi, rows, depth), b16), vm((hi, rows, depth), b16),
             vm((rows, depth), f32),
             vm((O, tp_size, rows, depth), b16),
-            vm((tp_size, rows, depth), f32),
-            vm((O, hi, rows, depth), f32),
-            vm((O, hi, rows, depth), b16), vm((O, hi, rows, depth), b16),
-            vm((O, hi, rows, depth), b16), vm((O, hi, rows, depth), b16),
-            vm((O, rows, depth), f32),
-            vm((O, rows, depth), b16), vm((O + 1, rows, depth), b16),
+            vm((O, tp_size * rows, width), b16),
+            vm((tp_size, rows, half), f32),
+            vm((2 * O, hi, rows, half), f32),
+            vm((2 * O, hi, rows, half), b16), vm((2 * O, hi, rows, half), b16),
+            vm((2 * O, hi - 1, rows, half), b16), vm((2 * O, hi - 1, rows, half), b16),
+            vm((2 * O, rows, half), f32),
+            vm((2, O, rows, half), b16), vm((2, O + 1, rows, half), b16),
             dma((12,)),
             dma((steps,)), dma((steps,)), dma((steps,)), dma((steps,)),
             dma, dma, dma, dma,
             dma, dma((hi - 1, F)),
             dma, dma((O, up_pieces)),
-            dma, dma, dma, dma,
+            dma, dma, dma, dma((2,)),
             dma((O, 2)), dma((O, F)),
             dma, dma((O, hi - 1, F)),
             dma, dma((O,)),
-            dma, dma((O,)), dma, dma((O, hi - 1, F)),
-            dma, dma((O + 1, F)),
+            dma, dma((2 * O,)), dma, dma((2 * O, hi - 1, C)),
+            dma, dma((2, O + 1, C)),
         ],
         compiler_params=pltpu.CompilerParams(
             collective_id=0, has_side_effects=True, vmem_limit_bytes=60 * 1024 * 1024

time: 86 us -> 82.3 us (0.957); the launches traced: 85 us -> 82.2 us
  Pallas kernels: 83.3 us -> 80.5 us
    pallas_call x1, Pallas kernels: 83.3 us -> 80.5 us  [on_device(): pl.pallas_call(functools.partial(layer_kernel, sp_size, tp_size, up_piece...]
where the time goes in v3:
time: 82.3 us; the launch traced here: 82.2 us
  Pallas kernels  80.5 us (98%)
  local copies, waits for them, and re-layouts  1.67 us (2%)
    pallas_call x1, Pallas kernels, on_device(): pl.pallas_call(functools.partial(layer_kernel, sp_size, tp_size, up_piece...  80.5 us
    unnamed x1, local copies, waits for them, and re-layouts  1.67 us

profile of v3, /device:TPU:0, one launch (start us, length us, event | category | flops | bytes accessed | tf_op | source)
XLA Modules:
  0.0 82.2 jit_solution(6337183499710547537)
XLA Ops:
  0.0 80.5 %shard_map.118 = bf16[64,2048]{1,0:T(8,128)(2,1)} custom-call(bf16[256,256]{1,0:T(8,128)(2,1)} %q_hbm.1, bf16[256,256]{1,0:T(8,128)(2,1)} %f_hbm.1, bf16[256,256]{1,0:T(8,128)(2,1)} %v_hbm.1, bf16[256,256]{1,0:T(8,128)(2,1)} %g_hbm.1, f32[1,256]{1,0:T(1,128)} %bitcast.4, f32[256,256]{1,0:T(8,128)} %ex_hbm.1, f32[1,128]{1,0:T(1,128)} %bitcast.5, ...), custom_call_target="tpu_custom_call" | custom-call | tf_op jit(solution)/shard_map/pallas_call | solution.py:641
  80.5 1.7 %copy.14 = bf16[64,2048]{1,0:T(8,128)(2,1)} copy(bf16[64,2048]{1,0:T(8,128)(2,1)} %shard_map.118) | data formatting | bytes 524288

commit v4 on v3

--- a/solution.py
+++ b/solution.py
@@ -447,6 +447,10 @@
         for q in range(fine):
             gather(chunk_at(outer - 1), q)
 
+    @pl.when(o + 1 < outer)
+    def _():
+        gather_last()
+
     for c in loads[10:]:
         c.wait()
     fw_all.wait_recv()
@@ -535,7 +539,9 @@
         @pl.when(j == 1)
         def _():
             send_sums(0)
-            gather_last()
+            @pl.when(o + 1 == outer)
+            def _():
+                gather_last()
 
         @pl.when(j < slots)
         def _():

time: 82.3 us -> 81.1 us (0.985)
  Pallas kernels: 80.5 us -> 79.3 us
    pallas_call x1, Pallas kernels: 80.5 us -> 79.3 us  [on_device(): pl.pallas_call(functools.partial(layer_kernel, sp_size, tp_size, up_piece...]
where the time goes in v4:
time: 81.1 us; the launch traced here: 81 us
  Pallas kernels  79.3 us (98%)
  local copies, waits for them, and re-layouts  1.67 us (2%)
    pallas_call x1, Pallas kernels, on_device(): pl.pallas_call(functools.partial(layer_kernel, sp_size, tp_size, up_piece...  79.3 us
    unnamed x1, local copies, waits for them, and re-layouts  1.67 us

profile of v4, /device:TPU:0, one launch (start us, length us, event | category | flops | bytes accessed | tf_op | source)
XLA Modules:
  0.0 81.0 jit_solution(2314241156425898926)
XLA Ops:
  0.0 79.3 %shard_map.118 = bf16[64,2048]{1,0:T(8,128)(2,1)} custom-call(bf16[256,256]{1,0:T(8,128)(2,1)} %q_hbm.1, bf16[256,256]{1,0:T(8,128)(2,1)} %f_hbm.1, bf16[256,256]{1,0:T(8,128)(2,1)} %v_hbm.1, bf16[256,256]{1,0:T(8,128)(2,1)} %g_hbm.1, f32[1,256]{1,0:T(1,128)} %bitcast.4, f32[256,256]{1,0:T(8,128)} %ex_hbm.1, f32[1,128]{1,0:T(1,128)} %bitcast.5, ...), custom_call_target="tpu_custom_call" | custom-call | tf_op jit(solution)/shard_map/pallas_call | solution.py:647
  79.3 1.7 %copy.14 = bf16[64,2048]{1,0:T(8,128)(2,1)} copy(bf16[64,2048]{1,0:T(8,128)(2,1)} %shard_map.118) | data formatting | bytes 524288

commit v5 on v4

--- a/solution.py
+++ b/solution.py
@@ -427,7 +427,7 @@
 
     @pl.when(o == 0)
     def _():
-        up_issue(rising_far)
+        up_issue(rising_far[:2])
 
     for p in range(1, outer):
         c = chunk_at(p)
@@ -437,6 +437,10 @@
             spread(c, q)
             gather(chunk_at(p - 1), q)
             if p == 1 and q == 0:
+                @pl.when(o == 0)
+                def _():
+                    up_issue(rising_far[2:])
+
                 fw_issue(near)
             if p == 1 and q == fine // 2:
                 fw_issue([it for it in far if it[0] > 0])

time: 81.1 us -> 81.1 us (level)
  no operation moved by 1% of the time
where the time goes in v5:
time: 81.1 us; the launch traced here: 81 us
  Pallas kernels  79.3 us (98%)
  local copies, waits for them, and re-layouts  1.67 us (2%)
    pallas_call x1, Pallas kernels, on_device(): pl.pallas_call(functools.partial(layer_kernel, sp_size, tp_size, up_piece...  79.3 us
    unnamed x1, local copies, waits for them, and re-layouts  1.67 us

profile of v5, /device:TPU:0, one launch (start us, length us, event | category | flops | bytes accessed | tf_op | source)
XLA Modules:
  0.0 81.0 jit_solution(3277338366742721508)
XLA Ops:
  0.0 79.3 %shard_map.118 = bf16[64,2048]{1,0:T(8,128)(2,1)} custom-call(bf16[256,256]{1,0:T(8,128)(2,1)} %q_hbm.1, bf16[256,256]{1,0:T(8,128)(2,1)} %f_hbm.1, bf16[256,256]{1,0:T(8,128)(2,1)} %v_hbm.1, bf16[256,256]{1,0:T(8,128)(2,1)} %g_hbm.1, f32[1,256]{1,0:T(1,128)} %bitcast.4, f32[256,256]{1,0:T(8,128)} %ex_hbm.1, f32[1,128]{1,0:T(1,128)} %bitcast.5, ...), custom_call_target="tpu_custom_call" | custom-call | tf_op jit(solution)/shard_map/pallas_call | solution.py:651
  79.3 1.7 %copy.14 = bf16[64,2048]{1,0:T(8,128)(2,1)} copy(bf16[64,2048]{1,0:T(8,128)(2,1)} %shard_map.118) | data formatting | bytes 524288
